TPU v7x, 32 devices: a whole 2x2x4 slice. The times are simulated.
32 devices in a mesh: grp: 2 (over y), sp: 4 (over z), tp: 4 (over x, core).
Axes of the slice: x: 2, y: 2, z: 4, core: 2. Of those that a mesh axis runs over, the one named last changes fastest.
Arguments:
- tokens: bfloat16 [2048, 4096], P(('grp', 'sp'), 'tp'), parts along dimension 0, may hold values from -45 to 45
- norm_gain: float32 [2, 4096], replicated, may hold values from 0.1 to 1.9
- value_weight: bfloat16 [2, 4096, 1024], P(None, 'sp', 'tp'), may hold values from -0.09375 to 0.09375
- gate_weight: bfloat16 [2, 4096, 1024], P(None, 'sp', 'tp'), may hold values from -0.09375 to 0.09375
- conv_taps: float32 [2, 31, 1024], P(None, None, 'tp'), may hold values from -4 to 4
- channel_gain: float32 [2, 1024], P(None, 'tp'), may hold values from 0.1 to 1.9
- out_weight: bfloat16 [2, 1024, 4096], P(None, 'sp', 'tp'), may hold values from -0.375 to 0.375
- final_gain: float32 [4096], P('tp'), may hold values from 0.1 to 1.9
Outputs:
- result: bfloat16 [2048, 4096], P(('grp', 'sp'), 'tp'), parts along dimension 0
There are 2 independent parts, one for each index of `grp`. A program takes and returns all parts, laid end to end along the dimension named above; an argument that names none is the same for every part. Nothing has to cross between parts.
All inputs are finite; a program needn't handle non-finite values.
Results may differ from a plain program's by a relative error of at most 0.012.
Values may be sent and summed in bfloat16 or wider, within the bound.
A program may use at most 128 MiB of HBM per device.

v0:
```python
import functools

import jax
import jax.numpy as jnp
from jax import lax
from jax.experimental import pallas as pl
from jax.experimental.pallas import tpu as pltpu
from jax.sharding import PartitionSpec as P

MESH = pl.DeviceIdType.MESH
Q = 2
PAD = 16


def kernel(
    G, n, T, L,
    tokens, gain, value_w, gate_w, taps, cgain, out_w, fgain,
    result,
    wvg, wo, xg, xn, glu_out, acc, pad, padf, conv, stat, actg, x_state,
    local_sem, z_recv, right_send, left_send, y_send, y_recv,
    x_send, x_recv, a_send, a_recv, s_send, s_recv, h_send, h_recv, f_send, f_recv,
):
    g, s, t = lax.axis_index("grp"), lax.axis_index("sp"), lax.axis_index("tp")
    rows, width = tokens.shape
    depth, chans = value_w.shape[1:]
    out_rows = out_w.shape[1]
    half = chans // G
    out_half = width // G
    reach = taps.shape[1] // 2
    n_taps = taps.shape[1]
    D = width * T
    C = chans * T
    chunk = depth // Q
    pieces = Q + 1
    f32, bf16 = jnp.float32, jnp.bfloat16
    helped = n >= 4
    last = n - 1
    is_end = (s == 0) | (s == last)
    helper = (s == 1) | (s == last - 1)
    end = jnp.where(s == 1, 0, last)
    inward = jnp.where(s == 0, 1, last - 1)

    def ends_out(p):
        return helped and p < Q

    def to_right_ok(p):
        return s < last - 1 if ends_out(p) else s < last

    def to_left_ok(p):
        return s > 1 if ends_out(p) else s > 0

    def takes(p):
        return jnp.logical_not(is_end) if ends_out(p) else s >= 0

    def by_grp(p, j):
        ok = takes(p) & (j != s)
        if helped and p == 0:
            ok = ok & jnp.logical_not((s == 1) & (j == 0)) & jnp.logical_not((s == last - 1) & (j == last))
        return ok

    def piece(p, h, j):
        layer, q = p // pieces, p % pieces
        if q < Q:
            start = pl.multiple_of(j * depth + q * chunk, chunk)
            return wvg.at[layer, h, pl.ds(start, chunk), :]
        return wo.at[layer, h, pl.ds(pl.multiple_of(j * out_rows, out_rows), out_rows), :]

    locals_ = [pltpu.make_async_copy(tokens, xg.at[0, t], local_sem.at[0])]
    own_rows = pl.ds(pl.multiple_of(s * depth, depth), depth)
    own_out = pl.ds(pl.multiple_of(s * out_rows, out_rows), out_rows)
    count = 1
    per_layer = []
    for layer in range(L):
        group = []
        for h in range(G):
            for k, w in enumerate((value_w, gate_w)):
                group.append(pltpu.make_async_copy(
                    w.at[layer, :, pl.ds(h * half, half)],
                    wvg.at[layer, h, own_rows, pl.ds(k * half, half)],
                    local_sem.at[count]))
                count += 1
            group.append(pltpu.make_async_copy(
                out_w.at[layer, :, pl.ds(h * out_half, out_half)],
                wo.at[layer, h, own_out, :], local_sem.at[count]))
            count += 1
        per_layer.append(group)
    for c in locals_ + sum(per_layer, []):
        c.start()

    barrier = pltpu.get_barrier_semaphore()
    for d in range(1, T):
        pl.semaphore_signal(barrier, inc=1, device_id={"tp": lax.rem(t + d, T)}, device_id_type=MESH)
    for d in range(1, G):
        pl.semaphore_signal(barrier, inc=1, device_id={"grp": lax.rem(g + d, G)}, device_id_type=MESH)

    @pl.when(s > 0)
    def _():
        pl.semaphore_signal(barrier, inc=1, device_id={"sp": s - 1}, device_id_type=MESH)

    @pl.when(s < n - 1)
    def _():
        pl.semaphore_signal(barrier, inc=1, device_id={"sp": s + 1}, device_id_type=MESH)

    sides = jnp.where(s > 0, 1, 0) + jnp.where(s < n - 1, 1, 0)
    pl.semaphore_wait(barrier, (T - 1) + (G - 1) + sides)

    def right(p, j):
        r = piece(p, g, j)
        return pltpu.make_async_remote_copy(
            src_ref=r, dst_ref=r, send_sem=right_send.at[p, j], recv_sem=z_recv.at[p, j],
            device_id={"sp": s + 1}, device_id_type=MESH)

    def left(p, j):
        r = piece(p, g, j)
        return pltpu.make_async_remote_copy(
            src_ref=r, dst_ref=r, send_sem=left_send.at[p, j], recv_sem=z_recv.at[p, j],
            device_id={"sp": s - 1}, device_id_type=MESH)

    def across(p, j, d, h):
        r = piece(p, h, j)
        return pltpu.make_async_remote_copy(
            src_ref=r, dst_ref=r, send_sem=y_send.at[p, j, d - 1], recv_sem=y_recv.at[p, j, d - 1],
            device_id={"grp": lax.rem(g + d, G)}, device_id_type=MESH)

    batches = []
    for layer in range(L):
        base = layer * pieces
        batches += [list(range(base, base + Q)), [base + Q]]

    def own_right(ps):
        for p in ps:
            right(p, s).start()

    def own_left(ps):
        for p in ps:
            left(p, s).start()

    def end_rows(target):
        return pltpu.make_async_remote_copy(
            src_ref=xg.at[0, t], dst_ref=xg.at[L, t], send_sem=f_send.at[0], recv_sem=f_recv.at[0],
            device_id={"sp": target}, device_id_type=MESH)

    def end_piece(d, h, j, target):
        r = piece(0, h, j)
        return pltpu.make_async_remote_copy(
            src_ref=r, dst_ref=r, send_sem=f_send.at[d], recv_sem=f_recv.at[d],
            device_id={"sp": target}, device_id_type=MESH)

    def end_glu(target):
        return pltpu.make_async_remote_copy(
            src_ref=glu_out, dst_ref=pad.at[0, pl.ds(PAD, rows), :],
            send_sem=f_send.at[G], recv_sem=f_recv.at[G],
            device_id={"sp": target}, device_id_type=MESH)

    def relay(b, low, high):
        low, high = min(low, n - 1), min(high, n - 1)
        following = batches[b + 1] if b + 1 < len(batches) else []

        def step(k, carry):
            for p in batches[b]:
                from_left, from_right = s - 1 - k, s + 1 + k

                @pl.when((from_left >= 0) & takes(p))
                def _():
                    j = jnp.maximum(from_left, 0)
                    right(p, j).wait_recv()

                    @pl.when(to_right_ok(p))
                    def _():
                        right(p, j).start()

                    @pl.when(by_grp(p, j))
                    def _():
                        for d in range(1, G):
                            across(p, j, d, g).start()

                @pl.when((from_right < n) & takes(p))
                def _():
                    j = jnp.minimum(from_right, n - 1)
                    left(p, j).wait_recv()

                    @pl.when(to_left_ok(p))
                    def _():
                        left(p, j).start()

                    @pl.when(by_grp(p, j))
                    def _():
                        for d in range(1, G):
                            across(p, j, d, g).start()

            @pl.when((k == s - 1) & (s < (last - 1 if helped and b < 2 else last)))
            def _():
                own_right(following)

            @pl.when((k == n - 2 - s) & (s > (1 if helped and b < 2 else 0)))
            def _():
                own_left(following)

            return carry

        if high > low:
            lax.fori_loop(low, high, step, 0)

    def wait_across(b):
        for p in batches[b]:
            def step(j, carry):
                @pl.when(by_grp(p, j))
                def _():
                    for d in range(1, G):
                        across(p, j, d, lax.rem(g + G - d, G)).wait_recv()
                return carry
            lax.fori_loop(0, n, step, 0)

    def spread(buf, layer, send, recv):
        def copy(bit, m):
            block = buf.at[layer, t ^ m]
            return pltpu.make_async_remote_copy(
                src_ref=block, dst_ref=block, send_sem=send.at[layer, bit + m], recv_sem=recv.at[layer, bit + m],
                device_id={"tp": t ^ bit}, device_id_type=MESH)

        def arrival(bit, m):
            block = buf.at[layer, t ^ bit ^ m]
            return pltpu.make_async_remote_copy(
                src_ref=block, dst_ref=block, send_sem=send.at[layer, bit + m], recv_sem=recv.at[layer, bit + m],
                device_id={"tp": t ^ bit}, device_id_type=MESH)

        bits = []
        bit = T // 2
        while bit >= 1:
            bits.append(bit)
            bit //= 2

        def begin():
            for bit in bits:
                copy(bit, 0).start()

        def finish():
            have, sent = [0], []
            for i, bit in enumerate(bits):
                for m in have:
                    arrival(bit, m).wait_recv()
                    sent.append((bit, m))
                    for lower in bits[i + 1:]:
                        copy(lower, m ^ bit).start()
                have = have + [m ^ bit for m in have]
            return lambda: [copy(bit, m).wait_send() for bit, m in sent]

        return begin, finish

    def exchange(index, columns):
        lane = lax.broadcasted_iota(jnp.int32, (rows, 128), 1)
        tile = jnp.zeros((rows, 128), f32)
        for i, column in enumerate(columns):
            tile = jnp.where(lane == i, column, tile)
        stat[index, 0] = tile.T[:8, :]

        def copy(d):
            return pltpu.make_async_remote_copy(
                src_ref=stat.at[index, 0], dst_ref=stat.at[index, d],
                send_sem=s_send.at[index, d - 1], recv_sem=s_recv.at[index, d - 1],
                device_id={"tp": lax.rem(t + d, T)}, device_id_type=MESH)

        for d in range(1, T):
            copy(d).start()

        def total():
            for d in range(1, T):
                copy(d).wait_recv()
            sums = stat[index, 0]
            for d in range(1, T):
                sums = sums + stat[index, d]
            wide = jnp.concatenate([sums, jnp.zeros((120, rows), f32)], axis=0).T
            for d in range(1, T):
                copy(d).wait_send()
            return [wide[:, i:i + 1] for i in range(len(columns))]

        return total

    def normalize(layer, held, into):
        def squares(j, total):
            part = xg[held, j].astype(f32)
            return total + jnp.sum(part * part, axis=1, keepdims=True)
        mean = lax.fori_loop(0, T, squares, jnp.zeros((rows, 1), f32)) / D
        scale = lax.rsqrt(mean + 1e-06)

        def body(j, carry):
            xn[into, j] = (xg[held, j].astype(f32) * scale * gain[layer * T + j][None, :]).astype(bf16)
            return carry
        lax.fori_loop(0, T, body, 0)

    def project(layer, held, put):
        for h in range(G):
            def body(j, carry):
                block = wvg[layer, h, pl.ds(pl.multiple_of(j * width, width), width), :]
                part = jnp.dot(xn[held, j], block, preferred_element_type=f32)

                @pl.when(j == 0)
                def _():
                    acc[...] = part

                @pl.when(j > 0)
                def _():
                    acc[...] += part
                return carry
            lax.fori_loop(0, T, body, 0)
            glu = acc[:, :half] * jax.nn.sigmoid(acc[:, half:])
            put(h, glu.astype(bf16))

    for c in locals_:
        c.wait()
    spreads = [spread(xg, layer, x_send, x_recv) for layer in range(L)]
    spreads[0][0]()
    for c in sum(per_layer, []):
        c.wait()

    @pl.when(to_right_ok(0))
    def _():
        own_right(batches[0])

    @pl.when(to_left_ok(0))
    def _():
        own_left(batches[0])

    if helped:
        @pl.when(is_end)
        def _():
            end_rows(inward).start()
            for d in range(1, G):
                end_piece(d, lax.rem(g + d, G), s, inward).start()

        @pl.when(s == last - 1)
        def _():
            own_right(batches[1])
            if L > 1:
                own_right(batches[2])

        @pl.when(s == 1)
        def _():
            own_left(batches[1])
            if L > 1:
                own_left(batches[2])

    @pl.when((s == 0) & (s < n - 1))
    def _():
        for b in batches[1:]:
            own_right(b)

    @pl.when((s == n - 1) & (s > 0))
    def _():
        for b in batches[1:]:
            own_left(b)

    x_state[...] = tokens_f32(tokens, xg, t)
    drains = []

    for layer in range(L):
        first, second = 2 * layer, 2 * layer + 1
        if layer == 0:
            relay(first, 0, 1)
        else:
            relay(first, 1, 2)
        drains.append(spreads[layer][1]())
        if helped and layer == 0:
            @pl.when(jnp.logical_not(is_end))
            def _():
                normalize(layer, layer, 0)
        else:
            normalize(layer, layer, 0)
        relay(first, 1 if layer == 0 else 2, n)
        begin, finish = spread(xg, L, x_send, x_recv)
        if helped and layer == 0:
            @pl.when(helper)
            def _():
                end_rows(end).wait_recv()
                begin()

        relay(second, 0, 1)

        def put(h, value):
            pad[layer, PAD:PAD + rows, h * half:(h + 1) * half] = value

        def put_out(h, value):
            glu_out[:, h * half:(h + 1) * half] = value

        if helped and layer == 0:
            @pl.when(helper)
            def _():
                drain = finish()
                normalize(0, L, 1)
                for d in range(1, G):
                    end_piece(d, lax.rem(g + d, G), end, end).wait_recv()
                drain()

            wait_across(first)

            @pl.when(helper)
            def _():
                project(0, 1, put_out)
                end_glu(end).start()

            @pl.when(jnp.logical_not(is_end))
            def _():
                project(0, 0, put)

            @pl.when(helper)
            def _():
                end_glu(end).wait_send()

            @pl.when(is_end)
            def _():
                end_rows(inward).wait_send()
                for d in range(1, G):
                    end_piece(d, lax.rem(g + d, G), s, inward).wait_send()
                end_glu(inward).wait_recv()
        else:
            wait_across(first)
            project(layer, 0, put)

        def to_right():
            return pltpu.make_async_remote_copy(
                src_ref=pad.at[layer, pl.ds(rows, PAD), :], dst_ref=pad.at[layer, pl.ds(0, PAD), :],
                send_sem=h_send.at[layer, 0], recv_sem=h_recv.at[layer, 0],
                device_id={"sp": s + 1}, device_id_type=MESH)

        def to_left():
            return pltpu.make_async_remote_copy(
                src_ref=pad.at[layer, pl.ds(PAD, PAD), :], dst_ref=pad.at[layer, pl.ds(PAD + rows, PAD), :],
                send_sem=h_send.at[layer, 1], recv_sem=h_recv.at[layer, 1],
                device_id={"sp": s - 1}, device_id_type=MESH)

        @pl.when(s < n - 1)
        def _():
            to_right().start()

        @pl.when(s > 0)
        def _():
            to_left().start()

        @pl.when(s == 0)
        def _():
            pad[layer, 0:PAD, :] = jnp.zeros((PAD, chans), bf16)

        @pl.when(s == n - 1)
        def _():
            pad[layer, PAD + rows:, :] = jnp.zeros((PAD, chans), bf16)

        relay(second, 1, 2)

        @pl.when(s > 0)
        def _():
            to_right().wait_recv()

        @pl.when(s < n - 1)
        def _():
            to_left().wait_recv()

        padf[...] = pad[layer].astype(f32)
        block = 64
        sums, squares = [], []
        for r in range(0, rows, block):
            total = jnp.zeros((block, chans), f32)
            for k in range(n_taps):
                start = r + PAD - reach + k
                total = total + taps[layer, k][None, :] * padf[start:start + block, :]
            conv[r:r + block, :] = total
            sums.append(jnp.sum(total, axis=1, keepdims=True))
            squares.append(jnp.sum(total * total, axis=1, keepdims=True))
        totals = exchange(layer, [jnp.concatenate(sums, 0), jnp.concatenate(squares, 0)])
        relay(second, 2, n)
        if layer + 1 < L:
            relay(second + 1, 0, 1)
        total, square = totals()
        center = total / C
        spread_ = square / C - center * center
        normal = (conv[...] - center) * lax.rsqrt(spread_ + 1e-05)
        actg[layer, t] = jax.nn.silu(normal * cgain[layer][None, :]).astype(bf16)
        act_begin, act_finish = spread(actg, layer, a_send, a_recv)
        act_begin()
        drains.append(act_finish())
        wait_across(second)
        for h in range(G):
            part = None
            for j in range(T):
                term = jnp.dot(actg[layer, j], wo[layer, h, j * chans:(j + 1) * chans, :], preferred_element_type=f32)
                part = term if part is None else part + term
            cols = slice(h * out_half, (h + 1) * out_half)
            x_state[:, cols] = (x_state[:, cols] + part).astype(bf16).astype(f32)
        if layer + 1 < L:
            xg[layer + 1, t] = x_state[...].astype(bf16)
            spreads[layer + 1][0]()

        @pl.when(s < n - 1)
        def _():
            to_right().wait_send()

        @pl.when(s > 0)
        def _():
            to_left().wait_send()

    xf = x_state[...]
    totals = exchange(L, [jnp.sum(xf * xf, axis=1, keepdims=True)])

    for drain in drains:
        drain()

    def drain_step(j, carry):
        for p in range(L * pieces):
            came = (j == s) | takes(p)

            @pl.when((j <= s) & to_right_ok(p) & came)
            def _():
                right(p, j).wait_send()

            @pl.when((j >= s) & to_left_ok(p) & came)
            def _():
                left(p, j).wait_send()

            @pl.when(by_grp(p, j))
            def _():
                for d in range(1, G):
                    across(p, j, d, g).wait_send()
        return carry
    lax.fori_loop(0, n, drain_step, 0)

    (total,) = totals()
    scale = lax.rsqrt(total / D + 1e-06)
    result[...] = (x_state[...] * scale * fgain[...]).astype(bf16)


def tokens_f32(tokens, xg, t):
    return xg[0, t].astype(jnp.float32)


def on_device(G, n, T, tokens, norm_gain, value_w, gate_w, taps, cgain, out_w, fgain):
    L = norm_gain.shape[0]
    rows, width = tokens.shape
    depth, chans = value_w.shape[1:]
    D, C = width * T, chans * T
    bf16, f32 = jnp.bfloat16, jnp.float32
    dma = pltpu.SemaphoreType.DMA
    vmem = pl.BlockSpec(memory_space=pltpu.VMEM)
    hbm = pl.BlockSpec(memory_space=pl.ANY)
    P_ = L * (Q + 1)
    peers = max(G - 1, 1)
    return pl.pallas_call(
        functools.partial(kernel, G, n, T, L),
        out_shape=jax.ShapeDtypeStruct((rows, width), bf16),
        in_specs=[hbm, vmem, hbm, hbm, vmem, vmem, hbm, vmem],
        out_specs=vmem,
        scratch_shapes=[
            pltpu.VMEM((L, G, D, 2 * chans // G), bf16),
            pltpu.VMEM((L, G, C, width // G), bf16),
            pltpu.VMEM((L + 1, T, rows, width), bf16),
            pltpu.VMEM((2, T, rows, width), bf16),
            pltpu.VMEM((rows, chans), bf16),
            pltpu.VMEM((rows, 2 * chans // G), f32),
            pltpu.VMEM((L, rows + 2 * PAD, chans), bf16),
            pltpu.VMEM((rows + 2 * PAD, chans), f32),
            pltpu.VMEM((rows, chans), f32),
            pltpu.VMEM((L + 1, T, 8, rows), f32),
            pltpu.VMEM((L, T, rows, chans), bf16),
            pltpu.VMEM((rows, width), f32),
            dma((1 + L * G * 3,)),
            dma((P_, n)), dma((P_, n)), dma((P_, n)),
            dma((P_, n, peers)), dma((P_, n, peers)),
            dma((L + 1, T)), dma((L + 1, T)), dma((L, T)), dma((L, T)),
            dma((L + 1, T)), dma((L + 1, T)),
            dma((L, 2)), dma((L, 2)),
            dma((G + 1,)), dma((G + 1,)),
        ],
        compiler_params=pltpu.CompilerParams(
            collective_id=0, has_side_effects=True, vmem_limit_bytes=56 * 2**20
        ),
    )(tokens, norm_gain.reshape(L * T, width), value_w, gate_w, taps, cgain, out_w, fgain.reshape(1, width))


def solution(mesh):
    placed = (
        P(("grp", "sp"), "tp"),
        P(),
        P(None, "sp", "tp"),
        P(None, "sp", "tp"),
        P(None, None, "tp"),
        P(None, "tp"),
        P(None, "sp", "tp"),
        P("tp"),
    )
    G, n, T = (mesh.shape[a] for a in ("grp", "sp", "tp"))
    return jax.shard_map(
        functools.partial(on_device, G, n, T),
        mesh=mesh, in_specs=placed, out_specs=P(("grp", "sp"), "tp"), check_vma=False,
    )
```

profile of v0, /device:TPU:0, one launch (start us, length us, event | category | flops | bytes accessed | tf_op | source)
XLA Modules:
  0.0 126.3 jit_solution(18178985592606857339)
XLA Ops:
  0.0 0.0 copy-start
  0.0 1.4 %reshape.6.gain = f32[8,1024]{1,0:T(8,128)} reshape(f32[2,4096]{1,0:T(2,128)} %param.9) | data formatting | bytes 65536 | tf_op jit(solution)/shard_map/reshape | solution.py:574
  1.4 0.0 copy-done
  1.4 0.6 copy.9.taps
  2.0 122.3 %shard_map.82 = bf16[256,1024]{1,0:T(8,128)(2,1)} custom-call(bf16[256,1024]{1,0:T(8,128)(2,1)} %tokens.1, f32[8,1024]{1,0:T(8,128)} %reshape.6.gain, bf16[2,1024,256]{2,1,0:T(8,128)(2,1)} %value_w.1, bf16[2,1024,256]{2,1,0:T(8,128)(2,1)} %gate_w.1, f32[2,31,256]{2,1,0:T(8,128)} %copy.9.taps, f32[2,256]{1,0:T(2,128)} %cgain.1, bf16[2,256,1024]{2,1,0:T(8,128)(2,1)} %out_w.1, ...), custom_call_target="tpu_custom_call" | custom-call | tf_op jit(solution)/shard_map/pallas_call | solution.py:545
  124.4 1.9 %copy.11 = bf16[256,1024]{1,0:T(8,128)(2,1)} copy(bf16[256,1024]{1,0:T(8,128)(2,1)} %shard_map.82) | data formatting | bytes 1048576
Async XLA Ops:
  0.0 1.4 %copy-start = (f32[2,31,256]{2,0,1:T(2,128)S(1)}, f32[2,31,256]{2,0,1:T(2,128)}, u32[]{:S(2)}) copy-start(f32[2,31,256]{2,0,1:T(2,128)} %param.12) | copy-start | bytes 190468
where the time goes:
time: 127 us; the launch traced here: 126 us
  Pallas kernels  122 us (96%)
  local copies, waits for them, and re-layouts  3.91 us (3%)
    pallas_call x1, Pallas kernels, on_device(): pl.pallas_call(functools.partial(kernel, G, n, T, L), out_shape=jax.Shape...  122 us

commit v1 on v0

--- a/solution.py
+++ b/solution.py
@@ -525,6 +525,606 @@
     (total,) = totals()
     scale = lax.rsqrt(total / D + 1e-06)
     result[...] = (x_state[...] * scale * fgain[...]).astype(bf16)
+
+
+QC = 4
+RC = 2
+
+
+def quad_kernel(
+    G, n, T, L,
+    tokens, gain, value_w, gate_w, taps, cgain, out_w, fgain,
+    result,
+    wvg, wo, xg, xn, glu_out, acc, pad, padf, conv, stat, actg, x_state,
+    local_sem, recv_z, recv_o, send_in, send_out, send_y, send_un,
+    x_send, x_recv, e_send, e_recv, a_send, a_recv, s_send, s_recv, h_send, h_recv, f_send, f_recv,
+):
+    g, s, t = lax.axis_index("grp"), lax.axis_index("sp"), lax.axis_index("tp")
+    rows, width = tokens.shape
+    depth, chans = value_w.shape[1:]
+    out_rows = out_w.shape[1]
+    half = chans // G
+    out_half = width // G
+    reach = taps.shape[1] // 2
+    n_taps = taps.shape[1]
+    D = width * T
+    C = chans * T
+    pieces = QC + RC
+    size = {"vg": depth // QC, "wo": out_rows // RC}
+    count = {"vg": QC, "wo": RC}
+    shared_from = QC // 2
+    f32, bf16 = jnp.float32, jnp.bfloat16
+    last = n - 1
+    low = s < n // 2
+    is_end = (s == 0) | (s == last)
+    is_mid = jnp.logical_not(is_end)
+    inner = jnp.where(low, s + 1, s - 1)
+    outer = jnp.where(low, s - 1, s + 1)
+    edge, mine, near, far = (jnp.where(low, a, last - a) for a in (0, 1, n - 2, n - 1))
+    other = lax.rem(g + 1, G)
+    x_chunks = QC
+    x_rows = rows // x_chunks
+    first_vg, first_wo, second_vg, second_wo = (0, "vg"), (0, "wo"), (1, "vg"), (1, "wo")
+    after = (first_wo, second_vg, second_wo)
+
+    def index(stage, q):
+        layer, kind = stage
+        return layer * pieces + (0 if kind == "vg" else QC) + q
+
+    def piece(stage, q, h, j):
+        layer, kind = stage
+        step = size[kind]
+        per = depth if kind == "vg" else out_rows
+        ref = wvg if kind == "vg" else wo
+        return ref.at[layer, h, pl.ds(pl.multiple_of(j * per + q * step, step), step), :]
+
+    token_copy = pltpu.make_async_copy(tokens, xg.at[0, t], local_sem.at[0])
+    own_rows = pl.ds(pl.multiple_of(s * depth, depth), depth)
+    own_out = pl.ds(pl.multiple_of(s * out_rows, out_rows), out_rows)
+    staged = {}
+    slot = 1
+    for layer in range(L):
+        staged[layer, "vg"], staged[layer, "wo"] = [], []
+        for h in range(G):
+            for k, w in enumerate((value_w, gate_w)):
+                staged[layer, "vg"].append(pltpu.make_async_copy(
+                    w.at[layer, :, pl.ds(h * half, half)],
+                    wvg.at[layer, h, own_rows, pl.ds(k * half, half)],
+                    local_sem.at[slot]))
+                slot += 1
+        for h in range(G):
+            staged[layer, "wo"].append(pltpu.make_async_copy(
+                out_w.at[layer, :, pl.ds(h * out_half, out_half)],
+                wo.at[layer, h, own_out, :], local_sem.at[slot]))
+            slot += 1
+    for c in staged[first_vg]:
+        c.start()
+    token_copy.start()
+    for stage in after:
+        for c in staged[stage]:
+            c.start()
+
+    barrier = pltpu.get_barrier_semaphore()
+    for d in range(1, T):
+        pl.semaphore_signal(barrier, inc=1, device_id={"tp": lax.rem(t + d, T)}, device_id_type=MESH)
+    pl.semaphore_signal(barrier, inc=1, device_id={"grp": other}, device_id_type=MESH)
+
+    @pl.when(s > 0)
+    def _():
+        pl.semaphore_signal(barrier, inc=1, device_id={"sp": s - 1}, device_id_type=MESH)
+
+    @pl.when(s < last)
+    def _():
+        pl.semaphore_signal(barrier, inc=1, device_id={"sp": s + 1}, device_id_type=MESH)
+
+    sides = jnp.where(s > 0, 1, 0) + jnp.where(s < last, 1, 0)
+    pl.semaphore_wait(barrier, (T - 1) + (G - 1) + sides)
+
+    def along(stage, q, j, target, send):
+        r, p = piece(stage, q, g, j), index(stage, q)
+        return pltpu.make_async_remote_copy(
+            src_ref=r, dst_ref=r, send_sem=send.at[p, j], recv_sem=recv_z.at[p, j],
+            device_id={"sp": target}, device_id_type=MESH)
+
+    def inward(stage, q, j):
+        return along(stage, q, j, inner, send_in)
+
+    def outward(stage, q, j):
+        return along(stage, q, j, outer, send_out)
+
+    def across(stage, q, j, h):
+        r, p = piece(stage, q, h, j), index(stage, q)
+        return pltpu.make_async_remote_copy(
+            src_ref=r, dst_ref=r, send_sem=send_y.at[p, j], recv_sem=recv_o.at[p, j],
+            device_id={"grp": other}, device_id_type=MESH)
+
+    def direct(stage, q):
+        r, p = piece(stage, q, other, edge), index(stage, q)
+        return pltpu.make_async_remote_copy(
+            src_ref=r, dst_ref=r, send_sem=send_un.at[p], recv_sem=recv_o.at[p, edge],
+            device_id={"sp": inner}, device_id_type=MESH)
+
+    def end_rows(c, target):
+        part = pl.ds(pl.multiple_of(c * x_rows, x_rows), x_rows)
+        return pltpu.make_async_remote_copy(
+            src_ref=xg.at[0, t, part], dst_ref=xg.at[L, t, part], send_sem=f_send.at[c], recv_sem=f_recv.at[c],
+            device_id={"sp": target}, device_id_type=MESH)
+
+    def end_glu(target):
+        return pltpu.make_async_remote_copy(
+            src_ref=glu_out, dst_ref=pad.at[0], send_sem=f_send.at[x_chunks], recv_sem=f_recv.at[x_chunks],
+            device_id={"sp": target}, device_id_type=MESH)
+
+    def each(low_, high_, body):
+        def step(q, carry):
+            body(q)
+            return carry
+        lax.fori_loop(low_, high_, step, 0)
+
+    def on(condition, body):
+        pl.when(condition)(body)
+
+    def from_inner(stage, q, j):
+        def serve():
+            inward(stage, q, j).wait_recv()
+            if stage != first_vg:
+                @pl.when(is_mid)
+                def _():
+                    outward(stage, q, j).start()
+            across(stage, q, j, g).start()
+        if stage == first_vg:
+            on(is_mid, serve)
+        else:
+            serve()
+
+    def from_edge(stage, q):
+        @pl.when(is_mid)
+        def _():
+            inward(stage, q, edge).wait_recv()
+            inward(stage, q, edge).start()
+            if stage == first_vg:
+                @pl.when(q >= shared_from)
+                def _():
+                    across(stage, q, edge, g).start()
+
+    def push_in(stage, lo, hi):
+        @pl.when(is_mid)
+        def _():
+            each(lo, hi, lambda q: inward(stage, q, mine).start())
+
+    def wait_other(stage):
+        kind = stage[1]
+
+        def body(j):
+            @pl.when(j != s)
+            def _():
+                each(0, count[kind], lambda q: across(stage, q, j, other).wait_recv())
+        each(0, n, body)
+
+    def spread(view, send, recv):
+        def copy(bit, m):
+            block = view(t ^ m)
+            return pltpu.make_async_remote_copy(
+                src_ref=block, dst_ref=block, send_sem=send.at[bit + m], recv_sem=recv.at[bit + m],
+                device_id={"tp": t ^ bit}, device_id_type=MESH)
+
+        def arrival(bit, m):
+            block = view(t ^ bit ^ m)
+            return pltpu.make_async_remote_copy(
+                src_ref=block, dst_ref=block, send_sem=send.at[bit + m], recv_sem=recv.at[bit + m],
+                device_id={"tp": t ^ bit}, device_id_type=MESH)
+
+        bits = []
+        bit = T // 2
+        while bit >= 1:
+            bits.append(bit)
+            bit //= 2
+
+        def begin():
+            for bit in bits:
+                copy(bit, 0).start()
+
+        def order():
+            have = [0]
+            for i, bit in enumerate(bits):
+                for m in have:
+                    yield bit, m, bits[i + 1:]
+                have = have + [m ^ bit for m in have]
+
+        def finish():
+            for bit, m, lower in order():
+                arrival(bit, m).wait_recv()
+                for b in lower:
+                    copy(b, m ^ bit).start()
+
+        def drain():
+            for bit, m, _ in order():
+                copy(bit, m).wait_send()
+
+        return begin, finish, drain
+
+    def whole(buf, layer, send, recv):
+        return spread(lambda j: buf.at[layer, j], send.at[layer], recv.at[layer])
+
+    def edge_spread(c):
+        part = pl.ds(pl.multiple_of(c * x_rows, x_rows), x_rows)
+        return spread(lambda j: xg.at[L, j, part], e_send.at[c], e_recv.at[c])
+
+    def exchange(index_, columns):
+        lane = lax.broadcasted_iota(jnp.int32, (rows, 128), 1)
+        tile = jnp.zeros((rows, 128), f32)
+        for i, column in enumerate(columns):
+            tile = jnp.where(lane == i, column, tile)
+        stat[index_, 0] = tile.T[:8, :]
+
+        def copy(d):
+            return pltpu.make_async_remote_copy(
+                src_ref=stat.at[index_, 0], dst_ref=stat.at[index_, d],
+                send_sem=s_send.at[index_, d - 1], recv_sem=s_recv.at[index_, d - 1],
+                device_id={"tp": lax.rem(t + d, T)}, device_id_type=MESH)
+
+        for d in range(1, T):
+            copy(d).start()
+
+        def total():
+            for d in range(1, T):
+                copy(d).wait_recv()
+            sums = stat[index_, 0]
+            for d in range(1, T):
+                sums = sums + stat[index_, d]
+            wide = jnp.concatenate([sums, jnp.zeros((120, rows), f32)], axis=0).T
+            for d in range(1, T):
+                copy(d).wait_send()
+            return [wide[:, i:i + 1] for i in range(len(columns))]
+
+        return total
+
+    def normalize(layer, held, into):
+        def squares(j, total):
+            part = xg[held, j].astype(f32)
+            return total + jnp.sum(part * part, axis=1, keepdims=True)
+        mean = lax.fori_loop(0, T, squares, jnp.zeros((rows, 1), f32)) / D
+        scale = lax.rsqrt(mean + 1e-06)
+
+        def body(j, carry):
+            xn[into, j] = (xg[held, j].astype(f32) * scale * gain[layer * T + j][None, :]).astype(bf16)
+            return carry
+        lax.fori_loop(0, T, body, 0)
+
+    def project(layer, held, put):
+        for h in range(G):
+            def body(j, carry):
+                block = wvg[layer, h, pl.ds(pl.multiple_of(j * width, width), width), :]
+                part = jnp.dot(xn[held, j], block, preferred_element_type=f32)
+
+                @pl.when(j == 0)
+                def _():
+                    acc[...] = part
+
+                @pl.when(j > 0)
+                def _():
+                    acc[...] += part
+                return carry
+            lax.fori_loop(0, T, body, 0)
+            glu = acc[:, :half] * jax.nn.sigmoid(acc[:, half:])
+            put(h, glu.astype(bf16))
+
+    def to_right(layer):
+        return pltpu.make_async_remote_copy(
+            src_ref=pad.at[layer, pl.ds(rows, PAD), :], dst_ref=pad.at[layer, pl.ds(0, PAD), :],
+            send_sem=h_send.at[layer, 0], recv_sem=h_recv.at[layer, 0],
+            device_id={"sp": s + 1}, device_id_type=MESH)
+
+    def to_left(layer):
+        return pltpu.make_async_remote_copy(
+            src_ref=pad.at[layer, pl.ds(PAD, PAD), :], dst_ref=pad.at[layer, pl.ds(PAD + rows, PAD), :],
+            send_sem=h_send.at[layer, 1], recv_sem=h_recv.at[layer, 1],
+            device_id={"sp": s - 1}, device_id_type=MESH)
+
+    def sides_of(layer):
+        if layer == 0:
+            return s == 1, s == last - 1, s == last - 1, s == 1
+        return s < last, s > 0, s > 0, s < last
+
+    def convolve(layer):
+        padf[...] = pad[layer].astype(f32)
+        block = 64
+        sums, squares = [], []
+        for r in range(0, rows, block):
+            total = jnp.zeros((block, chans), f32)
+            for k in range(n_taps):
+                start = r + PAD - reach + k
+                total = total + taps[layer, k][None, :] * padf[start:start + block, :]
+            conv[r:r + block, :] = total
+            sums.append(jnp.sum(total, axis=1, keepdims=True))
+            squares.append(jnp.sum(total * total, axis=1, keepdims=True))
+        return exchange(layer, [jnp.concatenate(sums, 0), jnp.concatenate(squares, 0)])
+
+    def activate(layer, totals):
+        total, square = totals()
+        center = total / C
+        spread_ = square / C - center * center
+        normal = (conv[...] - center) * lax.rsqrt(spread_ + 1e-05)
+        actg[layer, t] = jax.nn.silu(normal * cgain[layer][None, :]).astype(bf16)
+
+    def add_branch(layer):
+        for h in range(G):
+            part = None
+            for j in range(T):
+                term = jnp.dot(actg[layer, j], wo[layer, h, j * chans:(j + 1) * chans, :], preferred_element_type=f32)
+                part = term if part is None else part + term
+            cols = slice(h * out_half, (h + 1) * out_half)
+            x_state[:, cols] = (x_state[:, cols] + part).astype(bf16).astype(f32)
+
+    for c in staged[first_vg]:
+        c.wait()
+    on(s >= 0, lambda: each(0, QC, lambda q: inward(first_vg, q, s).start()))
+    token_copy.wait()
+    x_own = [whole(xg, layer, x_send, x_recv) for layer in range(L)]
+
+    @pl.when(is_end)
+    def _():
+        each(0, x_chunks, lambda c: end_rows(c, inner).start())
+
+    @pl.when(is_mid)
+    def _():
+        x_own[0][0]()
+
+    for stage in after:
+        for c in staged[stage]:
+            c.wait()
+
+    @pl.when(is_end)
+    def _():
+        each(0, shared_from, lambda q: direct(first_vg, q).start())
+        for stage in after:
+            each(0, count[stage[1]], lambda q: inward(stage, q, edge).start())
+            each(0, count[stage[1]], lambda q: direct(stage, q).start())
+
+    @pl.when(is_mid)
+    def _():
+        for stage in after:
+            each(0, count[stage[1]], lambda q: outward(stage, q, mine).start())
+
+    x_state[...] = xg[0, t].astype(f32)
+
+    def first_chunks(q):
+        from_edge(first_vg, q)
+        from_inner(first_vg, q, near)
+    each(0, QC, first_chunks)
+
+    @pl.when(is_end)
+    def _():
+        def pass_on(stage):
+            def body(q):
+                outward(stage, q, mine).wait_recv()
+                across(stage, q, mine, g).start()
+            each(0, count[stage[1]], body)
+        for stage in after:
+            pass_on(stage)
+
+    @pl.when(is_mid)
+    def _():
+        x_own[0][1]()
+        normalize(0, 0, 0)
+
+    def second_chunks(q):
+        from_inner(first_vg, q, far)
+
+        @pl.when(is_mid)
+        def _():
+            end_rows(q, edge).wait_recv()
+            edge_spread(q)[0]()
+    each(0, QC, second_chunks)
+    push_in(first_wo, 0, RC)
+    push_in(second_vg, 0, QC // 2)
+    each(0, RC, lambda q: from_inner(first_wo, q, near))
+
+    def put(layer):
+        def store(h, value):
+            pad[layer, PAD:PAD + rows, h * half:(h + 1) * half] = value
+        return store
+
+    def put_out(h, value):
+        glu_out[PAD:PAD + rows, h * half:(h + 1) * half] = value
+
+    @pl.when(is_mid)
+    def _():
+        each(0, x_chunks, lambda c: edge_spread(c)[1]())
+        normalize(0, L, 1)
+        wait_other(first_vg)
+        project(0, 1, put_out)
+        project(0, 0, put(0))
+
+    sends_right, sends_left, from_left, from_right = sides_of(0)
+
+    @pl.when(sends_right)
+    def _():
+        to_right(0).start()
+        glu_out[0:PAD, :] = jnp.zeros((PAD, chans), bf16)
+        glu_out[PAD + rows:, :] = pad[0, PAD:2 * PAD, :]
+        pad[0, 0:PAD, :] = glu_out[rows:rows + PAD, :]
+
+    @pl.when(sends_left)
+    def _():
+        to_left(0).start()
+        glu_out[0:PAD, :] = pad[0, rows:rows + PAD, :]
+        glu_out[PAD + rows:, :] = jnp.zeros((PAD, chans), bf16)
+        pad[0, PAD + rows:, :] = glu_out[PAD:2 * PAD, :]
+
+    @pl.when(is_mid)
+    def _():
+        end_glu(edge).start()
+    each(0, RC, lambda q: from_edge(first_wo, q))
+    each(0, QC // 2, lambda q: from_inner(second_vg, q, near))
+    push_in(second_vg, QC // 2, QC)
+
+    @pl.when(from_left)
+    def _():
+        to_right(0).wait_recv()
+
+    @pl.when(from_right)
+    def _():
+        to_left(0).wait_recv()
+
+    @pl.when(is_end)
+    def _():
+        end_glu(inner).wait_recv()
+
+    totals = convolve(0)
+    each(0, RC, lambda q: from_inner(first_wo, q, far))
+    activate(0, totals)
+    act = [whole(actg, layer, a_send, a_recv) for layer in range(L)]
+    act[0][0]()
+    act[0][1]()
+    wait_other(first_wo)
+    add_branch(0)
+    xg[1, t] = x_state[...].astype(bf16)
+    x_own[1][0]()
+    each(QC // 2, QC, lambda q: from_inner(second_vg, q, near))
+
+    def third_chunks(q):
+        from_edge(second_vg, q)
+        from_inner(second_vg, q, far)
+    each(0, QC, third_chunks)
+    push_in(second_wo, 0, RC)
+    x_own[1][1]()
+    normalize(1, 1, 0)
+    each(0, RC, lambda q: from_inner(second_wo, q, near))
+    wait_other(second_vg)
+    project(1, 0, put(1))
+    sends_right, sends_left, from_left, from_right = sides_of(1)
+
+    @pl.when(sends_right)
+    def _():
+        to_right(1).start()
+
+    @pl.when(sends_left)
+    def _():
+        to_left(1).start()
+
+    @pl.when(jnp.logical_not(from_left))
+    def _():
+        pad[1, 0:PAD, :] = jnp.zeros((PAD, chans), bf16)
+
+    @pl.when(jnp.logical_not(from_right))
+    def _():
+        pad[1, PAD + rows:, :] = jnp.zeros((PAD, chans), bf16)
+
+    each(0, RC, lambda q: from_edge(second_wo, q))
+
+    @pl.when(from_left)
+    def _():
+        to_right(1).wait_recv()
+
+    @pl.when(from_right)
+    def _():
+        to_left(1).wait_recv()
+
+    totals = convolve(1)
+    each(0, RC, lambda q: from_inner(second_wo, q, far))
+    activate(1, totals)
+    act[1][0]()
+    act[1][1]()
+    wait_other(second_wo)
+    add_branch(1)
+    xf = x_state[...]
+    totals = exchange(L, [jnp.sum(xf * xf, axis=1, keepdims=True)])
+
+    for layer in range(L):
+        sends_right, sends_left, _, _ = sides_of(layer)
+
+        @pl.when(sends_right)
+        def _():
+            to_right(layer).wait_send()
+
+        @pl.when(sends_left)
+        def _():
+            to_left(layer).wait_send()
+    act[0][2]()
+    act[1][2]()
+    x_own[1][2]()
+
+    @pl.when(is_mid)
+    def _():
+        x_own[0][2]()
+        each(0, x_chunks, lambda c: edge_spread(c)[2]())
+        end_glu(edge).wait_send()
+        for stage in (first_vg,) + after:
+            def body(q):
+                inward(stage, q, mine).wait_send()
+                inward(stage, q, edge).wait_send()
+                if stage == first_vg:
+                    @pl.when(q >= shared_from)
+                    def _():
+                        across(stage, q, edge, g).wait_send()
+                for j in (near, far):
+                    across(stage, q, j, g).wait_send()
+                    if stage != first_vg:
+                        outward(stage, q, j).wait_send()
+                if stage != first_vg:
+                    outward(stage, q, mine).wait_send()
+            each(0, count[stage[1]], body)
+
+    @pl.when(is_end)
+    def _():
+        each(0, x_chunks, lambda c: end_rows(c, inner).wait_send())
+        each(0, shared_from, lambda q: direct(first_vg, q).wait_send())
+        each(0, QC, lambda q: inward(first_vg, q, edge).wait_send())
+        for stage in after:
+            def body(q):
+                inward(stage, q, edge).wait_send()
+                direct(stage, q).wait_send()
+                for j in (mine, near, far):
+                    across(stage, q, j, g).wait_send()
+            each(0, count[stage[1]], body)
+
+    (total,) = totals()
+    scale = lax.rsqrt(total / D + 1e-06)
+    result[...] = (x_state[...] * scale * fgain[...]).astype(bf16)
+
+
+def quad_on_device(G, n, T, tokens, norm_gain, value_w, gate_w, taps, cgain, out_w, fgain):
+    L = norm_gain.shape[0]
+    if L != 2:
+        return on_device(G, n, T, tokens, norm_gain, value_w, gate_w, taps, cgain, out_w, fgain)
+    rows, width = tokens.shape
+    depth, chans = value_w.shape[1:]
+    D, C = width * T, chans * T
+    bf16, f32 = jnp.bfloat16, jnp.float32
+    dma = pltpu.SemaphoreType.DMA
+    vmem = pl.BlockSpec(memory_space=pltpu.VMEM)
+    hbm = pl.BlockSpec(memory_space=pl.ANY)
+    P_ = L * (QC + RC)
+    return pl.pallas_call(
+        functools.partial(quad_kernel, G, n, T, L),
+        out_shape=jax.ShapeDtypeStruct((rows, width), bf16),
+        in_specs=[hbm, vmem, hbm, hbm, vmem, vmem, hbm, vmem],
+        out_specs=vmem,
+        scratch_shapes=[
+            pltpu.VMEM((L, G, D, 2 * chans // G), bf16),
+            pltpu.VMEM((L, G, C, width // G), bf16),
+            pltpu.VMEM((L + 1, T, rows, width), bf16),
+            pltpu.VMEM((2, T, rows, width), bf16),
+            pltpu.VMEM((rows + 2 * PAD, chans), bf16),
+            pltpu.VMEM((rows, 2 * chans // G), f32),
+            pltpu.VMEM((L, rows + 2 * PAD, chans), bf16),
+            pltpu.VMEM((rows + 2 * PAD, chans), f32),
+            pltpu.VMEM((rows, chans), f32),
+            pltpu.VMEM((L + 1, T, 8, rows), f32),
+            pltpu.VMEM((L, T, rows, chans), bf16),
+            pltpu.VMEM((rows, width), f32),
+            dma((1 + L * G * 3,)),
+            dma((P_, n)), dma((P_, n)), dma((P_, n)), dma((P_, n)), dma((P_, n)), dma((P_,)),
+            dma((L, T)), dma((L, T)), dma((QC, T)), dma((QC, T)), dma((L, T)), dma((L, T)),
+            dma((L + 1, T)), dma((L + 1, T)),
+            dma((L, 2)), dma((L, 2)),
+            dma((QC + 1,)), dma((QC + 1,)),
+        ],
+        compiler_params=pltpu.CompilerParams(
+            collective_id=0, has_side_effects=True, vmem_limit_bytes=56 * 2**20
+        ),
+    )(tokens, norm_gain.reshape(L * T, width), value_w, gate_w, taps, cgain, out_w, fgain.reshape(1, width))
 
 
 def tokens_f32(tokens, xg, t):
@@ -586,7 +1186,8 @@
         P("tp"),
     )
     G, n, T = (mesh.shape[a] for a in ("grp", "sp", "tp"))
+    paired = n - 2 == G == 2 and T & (T - 1) == 0
     return jax.shard_map(
-        functools.partial(on_device, G, n, T),
+        functools.partial(quad_on_device if paired else on_device, G, n, T),
         mesh=mesh, in_specs=placed, out_specs=P(("grp", "sp"), "tp"), check_vma=False,
     )

time: 127 us -> 122 us (0.961)
  Pallas kernels: 122 us -> 118 us
    pallas_call x1, Pallas kernels: 122 us -> 118 us  [quad_on_device(): pl.pallas_call(functools.partial(quad_kernel, G, n, T, L), out_shape=jax....]
where the time goes in v1:
time: 122 us
  Pallas kernels  118 us (97%)
  local copies, waits for them, and re-layouts  3.91 us (3%)
    pallas_call x1, Pallas kernels, quad_on_device(): pl.pallas_call(functools.partial(quad_kernel, G, n, T, L), out_shape=jax....  118 us
    unnamed x4, local copies, waits for them, and re-layouts  2.51 us

profile of v1, /device:TPU:0, one launch (start us, length us, event | category | flops | bytes accessed | tf_op | source)
XLA Modules:
  0.0 122.1 jit_solution(14942023092096760635)
XLA Ops:
  0.0 0.0 copy-start
  0.0 1.4 %reshape.6.gain = f32[8,1024]{1,0:T(8,128)} reshape(f32[2,4096]{1,0:T(2,128)} %param.9) | data formatting | bytes 65536 | tf_op jit(solution)/shard_map/reshape | solution.py:1127
  1.4 0.0 copy-done
  1.4 0.6 copy.9.taps
  2.0 118.2 %shard_map.82 = bf16[256,1024]{1,0:T(8,128)(2,1)} custom-call(bf16[256,1024]{1,0:T(8,128)(2,1)} %tokens.1, f32[8,1024]{1,0:T(8,128)} %reshape.6.gain, bf16[2,1024,256]{2,1,0:T(8,128)(2,1)} %value_w.1, bf16[2,1024,256]{2,1,0:T(8,128)(2,1)} %gate_w.1, f32[2,31,256]{2,1,0:T(8,128)} %copy.9.taps, f32[2,256]{1,0:T(2,128)} %cgain.1, bf16[2,256,1024]{2,1,0:T(8,128)(2,1)} %out_w.1, ...), custom_call_target="tpu_custom_call" | custom-call | tf_op jit(solution)/shard_map/pallas_call | solution.py:1099
  120.2 1.9 %copy.11 = bf16[256,1024]{1,0:T(8,128)(2,1)} copy(bf16[256,1024]{1,0:T(8,128)(2,1)} %shard_map.82) | data formatting | bytes 1048576
Async XLA Ops:
  0.0 1.4 %copy-start = (f32[2,31,256]{2,0,1:T(2,128)S(1)}, f32[2,31,256]{2,0,1:T(2,128)}, u32[]{:S(2)}) copy-start(f32[2,31,256]{2,0,1:T(2,128)} %param.12) | copy-start | bytes 190468

commit v2 on v0

--- a/solution.py
+++ b/solution.py
@@ -525,6 +525,724 @@
     (total,) = totals()
     scale = lax.rsqrt(total / D + 1e-06)
     result[...] = (x_state[...] * scale * fgain[...]).astype(bf16)
+
+
+QC = 4
+RC = 2
+
+
+def quad_kernel(
+    G, n, T, L,
+    tokens, gain_hbm, value_w, gate_w, taps_hbm, cgain_hbm, out_w, fgain_hbm,
+    result,
+    wvg, wo, xg, xn, glu_out, acc, pad, padf, convg, stat, x_state, gain, taps, cgain, fgain,
+    local_sem, recv_z, recv_o, send_w, x_sem, e_sem, c_sem, s_sem, h_sem, hs_sem, g_sem, f_sem,
+):
+    g, s, t = lax.axis_index("grp"), lax.axis_index("sp"), lax.axis_index("tp")
+    rows, width = tokens.shape
+    depth, chans = value_w.shape[1:]
+    out_rows = out_w.shape[1]
+    half = chans // G
+    out_half = width // G
+    n_taps = taps.shape[0]
+    reach = n_taps // 2
+    D = width * T
+    C = chans * T
+    full = rows + 2 * PAD
+    pieces = QC + RC
+    size = {"vg": depth // QC, "wo": out_rows // RC}
+    count = {"vg": QC, "wo": RC}
+    shared_from = QC - 1
+    f32, bf16 = jnp.float32, jnp.bfloat16
+    last = n - 1
+    low = s < n // 2
+    is_end = (s == 0) | (s == last)
+    is_mid = jnp.logical_not(is_end)
+    inner = jnp.where(low, s + 1, s - 1)
+    outer = jnp.where(low, s - 1, s + 1)
+    edge, mine, near, far = (jnp.where(low, a, last - a) for a in (0, 1, n - 2, n - 1))
+    other = lax.rem(g + 1, G)
+    x_chunks = QC
+    x_rows = rows // x_chunks
+    own = pl.ds(PAD, rows)
+    first_vg, first_wo, second_vg, second_wo = (0, "vg"), (0, "wo"), (1, "vg"), (1, "wo")
+    after = (first_wo, second_vg, second_wo)
+    scope = jax.named_scope
+    IN, OUT, Y, YE, UN = range(5)
+
+    def index(stage, q):
+        layer, kind = stage
+        return layer * pieces + (0 if kind == "vg" else QC) + q
+
+    def order_of(stage):
+        return stage[0] * 2 + (0 if stage[1] == "vg" else 1)
+
+    def place(j):
+        return jnp.where(j == near, 1, jnp.where(j == far, 2, 0))
+
+    def piece(stage, q, h, j):
+        layer, kind = stage
+        step = size[kind]
+        per = depth if kind == "vg" else out_rows
+        ref = wvg if kind == "vg" else wo
+        return ref.at[layer, h, pl.ds(pl.multiple_of(j * per + q * step, step), step), :]
+
+    def wait_bytes(ref, sem):
+        pltpu.make_async_copy(ref, ref, sem).wait()
+
+    own_rows = pl.ds(pl.multiple_of(s * depth, depth), depth)
+    own_out = pl.ds(pl.multiple_of(s * out_rows, out_rows), out_rows)
+
+    def stage_in(stage):
+        layer, kind = stage
+        sem = local_sem.at[order_of(stage)]
+        for h in range(G):
+            if kind == "vg":
+                for k, w in enumerate((value_w, gate_w)):
+                    pltpu.make_async_copy(
+                        w.at[layer, :, pl.ds(h * half, half)],
+                        wvg.at[layer, h, own_rows, pl.ds(k * half, half)], sem).start()
+            else:
+                pltpu.make_async_copy(
+                    out_w.at[layer, :, pl.ds(h * out_half, out_half)],
+                    wo.at[layer, h, own_out, :], sem).start()
+
+    def staged(stage):
+        layer, kind = stage
+        ref = wvg.at[layer, :, own_rows] if kind == "vg" else wo.at[layer, :, own_out]
+        wait_bytes(ref, local_sem.at[order_of(stage)])
+
+    token_copy = pltpu.make_async_copy(tokens, xg.at[0, t, own], local_sem.at[2 * L])
+    gain_copy = pltpu.make_async_copy(cgain_hbm, cgain.at[t], local_sem.at[2 * L + 1])
+    small = [
+        pltpu.make_async_copy(gain_hbm, gain, local_sem.at[2 * L + 2]),
+        pltpu.make_async_copy(taps_hbm, taps, local_sem.at[2 * L + 3]),
+        pltpu.make_async_copy(fgain_hbm, fgain, local_sem.at[2 * L + 4]),
+    ]
+    stage_in(first_vg)
+    token_copy.start()
+    gain_copy.start()
+    for stage in after:
+        stage_in(stage)
+    for c in small:
+        c.start()
+
+    barrier = pltpu.get_barrier_semaphore()
+    for d in range(1, T):
+        pl.semaphore_signal(barrier, inc=1, device_id={"tp": lax.rem(t + d, T)}, device_id_type=MESH)
+    pl.semaphore_signal(barrier, inc=1, device_id={"grp": other}, device_id_type=MESH)
+
+    @pl.when(s > 0)
+    def _():
+        pl.semaphore_signal(barrier, inc=1, device_id={"sp": s - 1}, device_id_type=MESH)
+
+    @pl.when(s < last)
+    def _():
+        pl.semaphore_signal(barrier, inc=1, device_id={"sp": s + 1}, device_id_type=MESH)
+
+    blank = jnp.zeros((T, PAD, width), bf16)
+
+    @pl.when(s < n // 2)
+    def _():
+        xg[0, :, 0:PAD, :] = blank
+
+    @pl.when(s >= n // 2)
+    def _():
+        xg[0, :, PAD + rows:, :] = blank
+
+    @pl.when(s == 0)
+    def _():
+        xg[1, :, 0:PAD, :] = blank
+
+    @pl.when(s == last)
+    def _():
+        xg[1, :, PAD + rows:, :] = blank
+
+    sides = jnp.where(s > 0, 1, 0) + jnp.where(s < last, 1, 0)
+    pl.semaphore_wait(barrier, (T - 1) + (G - 1) + sides)
+
+    def arrived(stage, q, j):
+        wait_bytes(piece(stage, q, g, j), recv_z.at[index(stage, q), place(j)])
+
+    def inward(stage, q, j):
+        r, p = piece(stage, q, g, j), index(stage, q)
+        there = jnp.where(is_end, 0, jnp.where(j == mine, 1, 2))
+        return pltpu.make_async_remote_copy(
+            src_ref=r, dst_ref=r, send_sem=send_w.at[IN], recv_sem=recv_z.at[p, there],
+            device_id={"sp": inner}, device_id_type=MESH)
+
+    def outward(stage, q, j):
+        r, p = piece(stage, q, g, j), index(stage, q)
+        return pltpu.make_async_remote_copy(
+            src_ref=r, dst_ref=r, send_sem=send_w.at[OUT], recv_sem=recv_z.at[p, place(j)],
+            device_id={"sp": outer}, device_id_type=MESH)
+
+    def across(stage, q, j, send=Y):
+        r = piece(stage, q, g, j)
+        return pltpu.make_async_remote_copy(
+            src_ref=r, dst_ref=r, send_sem=send_w.at[send], recv_sem=recv_o.at[order_of(stage)],
+            device_id={"grp": other}, device_id_type=MESH)
+
+    def direct(stage, q):
+        r = piece(stage, q, other, edge)
+        return pltpu.make_async_remote_copy(
+            src_ref=r, dst_ref=r, send_sem=send_w.at[UN], recv_sem=recv_o.at[order_of(stage)],
+            device_id={"sp": inner}, device_id_type=MESH)
+
+    def others_arrived(stage):
+        layer, kind = stage
+        per = depth if kind == "vg" else out_rows
+        ref = wvg if kind == "vg" else wo
+        wait_bytes(ref.at[layer, 0, pl.ds(0, (n - 1) * per)], recv_o.at[order_of(stage)])
+
+    def end_rows(c, target):
+        src = pl.ds(pl.multiple_of(PAD + c * x_rows, PAD), x_rows)
+        return pltpu.make_async_remote_copy(
+            src_ref=xg.at[0, t, src], dst_ref=xg.at[L, t, src], send_sem=f_sem.at[0], recv_sem=f_sem.at[2 + c],
+            device_id={"sp": target}, device_id_type=MESH)
+
+    def end_glu(target):
+        return pltpu.make_async_remote_copy(
+            src_ref=glu_out, dst_ref=pad.at[0], send_sem=f_sem.at[1], recv_sem=f_sem.at[2 + x_chunks],
+            device_id={"sp": target}, device_id_type=MESH)
+
+    def each(low_, high_, body):
+        def step(q, carry):
+            body(q)
+            return carry
+        lax.fori_loop(low_, high_, step, 0)
+
+    def from_inner(stage, q, j):
+        def serve():
+            arrived(stage, q, j)
+            if stage != first_vg:
+                @pl.when(is_mid)
+                def _():
+                    outward(stage, q, j).start()
+            across(stage, q, j).start()
+        if stage == first_vg:
+            pl.when(is_mid)(serve)
+        else:
+            serve()
+
+    def from_edge(stage, q):
+        @pl.when(is_mid)
+        def _():
+            arrived(stage, q, edge)
+            inward(stage, q, edge).start()
+            if stage == first_vg:
+                @pl.when(q >= shared_from)
+                def _():
+                    across(stage, q, edge, YE).start()
+
+    def push_in(stage, lo, hi):
+        @pl.when(is_mid)
+        def _():
+            each(lo, hi, lambda q: inward(stage, q, mine).start())
+
+    class Spread:
+        def __init__(self, view, three, two, sems):
+            self.view, self.three, self.two, self.sems = view, three, two, sems
+
+        def copy(self, j, bit, k):
+            block = self.view(j)
+            return pltpu.make_async_remote_copy(
+                src_ref=block, dst_ref=block, send_sem=self.sems(2), recv_sem=self.sems(k),
+                device_id={"tp": t ^ bit}, device_id_type=MESH)
+
+        def begin(self):
+            self.copy(t, T // 2, 0).start()
+            self.copy(t, 1, 1).start()
+
+        def relay(self):
+            wait_bytes(self.view(t), self.sems(0))
+            self.copy(t ^ (T // 2), 1, 1).start()
+
+        def complete(self):
+            wait_bytes(self.two, self.sems(1))
+
+        def drain(self):
+            wait_bytes(self.three, self.sems(2))
+
+    def x_spread(layer):
+        return Spread(lambda j: xg.at[layer, j, own], xg.at[layer, pl.ds(0, 3), own], xg.at[layer, pl.ds(0, 2), own],
+                      lambda k: x_sem.at[layer, k])
+
+    def edge_spread(c):
+        part = pl.ds(pl.multiple_of(PAD + c * x_rows, PAD), x_rows)
+        return Spread(lambda j: xg.at[L, j, part], xg.at[L, pl.ds(0, 3), part], xg.at[L, pl.ds(0, 2), part],
+                      lambda k: e_sem.at[c, k])
+
+    def halo_spread(layer, side):
+        part = pl.ds(0 if side == 0 else PAD + rows, PAD)
+        return Spread(lambda j: xg.at[layer, j, part], xg.at[layer, pl.ds(0, 3), part], xg.at[layer, pl.ds(0, 2), part],
+                      lambda k: hs_sem.at[layer, side, k])
+
+    def conv_spread(layer, part_):
+        part = pl.ds(part_ * (rows // 2), rows // 2)
+        return Spread(lambda j: convg.at[layer, j, part], convg.at[layer, pl.ds(0, 3), part],
+                      convg.at[layer, pl.ds(0, 2), part], lambda k: c_sem.at[layer, part_, k])
+
+    def to_peers(buf, sem, k):
+        for d in range(1, T):
+            pltpu.make_async_remote_copy(
+                src_ref=buf.at[0], dst_ref=buf.at[d], send_sem=sem.at[k], recv_sem=sem.at[k + 1],
+                device_id={"tp": lax.rem(t + d, T)}, device_id_type=MESH).start()
+
+    def columns_of(index_):
+        wait_bytes(stat.at[index_, pl.ds(0, T - 1)], s_sem.at[2 * index_ + 1])
+        got = jnp.concatenate([stat[index_, d] for d in range(T)] + [jnp.zeros((128 - 8 * T, rows), f32)], axis=0)
+        return got.T
+
+    def share(index_, columns):
+        lane = lax.broadcasted_iota(jnp.int32, (rows, 128), 1)
+        tile = jnp.zeros((rows, 128), f32)
+        for i, column in enumerate(columns):
+            tile = jnp.where(lane == i, column, tile)
+        stat[index_, 0] = tile.T[:8, :]
+        to_peers(stat.at[index_], s_sem, 2 * index_)
+
+    def normalize(layer, held, into, start, size_):
+        def squares(j, total):
+            part = xg[held, j, start:start + size_, :].astype(f32)
+            return total + jnp.sum(part * part, axis=1, keepdims=True)
+        mean = lax.fori_loop(0, T, squares, jnp.zeros((size_, 1), f32)) / D
+        scale = lax.rsqrt(mean + 1e-06)
+
+        def body(j, carry):
+            by = gain[pl.ds(layer, 1), pl.ds(pl.multiple_of(j * width, width), width)]
+            xn[into, j, start:start + size_, :] = (
+                xg[held, j, start:start + size_, :].astype(f32) * scale * by).astype(bf16)
+            return carry
+        lax.fori_loop(0, T, body, 0)
+
+    def project(layer, held, start, size_, into):
+        for h in range(G):
+            def body(j, carry):
+                block = wvg[layer, h, pl.ds(pl.multiple_of(j * width, width), width), :]
+                part = jnp.dot(xn[held, j, start:start + size_, :], block, preferred_element_type=f32)
+
+                @pl.when(j == 0)
+                def _():
+                    acc[start:start + size_, :] = part
+
+                @pl.when(j > 0)
+                def _():
+                    acc[start:start + size_, :] += part
+                return carry
+            lax.fori_loop(0, T, body, 0)
+            glu = acc[start:start + size_, :half] * jax.nn.sigmoid(acc[start:start + size_, half:])
+            into[start:start + size_, h * half:(h + 1) * half] = glu.astype(bf16)
+
+    def x_right(layer):
+        return pltpu.make_async_remote_copy(
+            src_ref=xg.at[layer, t, pl.ds(rows, PAD)], dst_ref=xg.at[layer, t, pl.ds(0, PAD)],
+            send_sem=h_sem.at[layer, 0], recv_sem=h_sem.at[layer, 2],
+            device_id={"sp": s + 1}, device_id_type=MESH)
+
+    def x_left(layer):
+        return pltpu.make_async_remote_copy(
+            src_ref=xg.at[layer, t, pl.ds(PAD, PAD)], dst_ref=xg.at[layer, t, pl.ds(PAD + rows, PAD)],
+            send_sem=h_sem.at[layer, 1], recv_sem=h_sem.at[layer, 3],
+            device_id={"sp": s - 1}, device_id_type=MESH)
+
+    def sides_of(layer):
+        if layer == 0:
+            return s == 1, s == last - 1, s == last - 1, s == 1
+        return s < last, s > 0, s > 0, s < last
+
+    def halo(layer, do):
+        sends_right, sends_left, from_left, from_right = sides_of(layer)
+        if do == "send":
+            pl.when(sends_right)(lambda: x_right(layer).start())
+            pl.when(sends_left)(lambda: x_left(layer).start())
+        elif do == "begin":
+            @pl.when(from_left)
+            def _():
+                wait_bytes(xg.at[layer, t, pl.ds(0, PAD)], h_sem.at[layer, 2])
+                halo_spread(layer, 0).begin()
+
+            @pl.when(from_right)
+            def _():
+                wait_bytes(xg.at[layer, t, pl.ds(0, PAD)], h_sem.at[layer, 3])
+                halo_spread(layer, 1).begin()
+        elif do == "drain":
+            @pl.when(sends_right)
+            def _():
+                wait_bytes(xg.at[layer, t, pl.ds(0, PAD)], h_sem.at[layer, 0])
+
+            @pl.when(sends_left)
+            def _():
+                wait_bytes(xg.at[layer, t, pl.ds(0, PAD)], h_sem.at[layer, 1])
+            pl.when(from_left)(lambda: halo_spread(layer, 0).drain())
+            pl.when(from_right)(lambda: halo_spread(layer, 1).drain())
+        else:
+            pl.when(from_left)(lambda: getattr(halo_spread(layer, 0), do)())
+            pl.when(from_right)(lambda: getattr(halo_spread(layer, 1), do)())
+
+    def convolve(layer):
+        padf[...] = pad[layer].astype(f32)
+        block = 64
+        sums, squares = [], []
+        for r in range(0, rows, block):
+            total = jnp.zeros((block, chans), f32)
+            for k in range(n_taps):
+                start = r + PAD - reach + k
+                total = total + taps[k, layer:layer + 1, :] * padf[start:start + block, :]
+            mean = jnp.sum(total, axis=1, keepdims=True) / chans
+            shifted = total - mean
+            convg[layer, t, r:r + block, :] = shifted.astype(bf16)
+            sums.append(mean)
+            squares.append(jnp.sum(shifted * shifted, axis=1, keepdims=True))
+            if r + block == rows // 2:
+                conv_spread(layer, 0).begin()
+        share(layer, [jnp.concatenate(sums, 0), jnp.concatenate(squares, 0)])
+        conv_spread(layer, 1).begin()
+
+    def add_branch(layer):
+        got = columns_of(layer)
+        means = [got[:, 8 * d:8 * d + 1] for d in range(T)]
+        center = sum(means[1:], means[0]) / T
+        apart = [m - center for m in means]
+        square = sum((got[:, 8 * d + 1:8 * d + 2] + chans * (apart[d] * apart[d]) for d in range(T)), jnp.zeros((rows, 1), f32))
+        scale = lax.rsqrt(square / C + 1e-05)
+        parts = [None] * G
+        for d in range(T):
+            j = lax.rem(t + T - d, T)
+            by = cgain[j, layer:layer + 1, :]
+            normal = (convg[layer, j].astype(f32) + apart[d]) * scale
+            act = jax.nn.silu(normal * by).astype(bf16)
+            for h in range(G):
+                block = wo[layer, h, pl.ds(pl.multiple_of(j * chans, chans), chans), :]
+                term = jnp.dot(act, block, preferred_element_type=f32)
+                parts[h] = term if parts[h] is None else parts[h] + term
+        for h in range(G):
+            cols = slice(h * out_half, (h + 1) * out_half)
+            x_state[:, cols] = (x_state[:, cols] + parts[h]).astype(bf16).astype(f32)
+
+    with scope("stage_wait"):
+        staged(first_vg)
+    token_copy.wait()
+    halo(0, "send")
+    each(0, QC, lambda q: inward(first_vg, q, s).start())
+
+    @pl.when(is_end)
+    def _():
+        each(0, x_chunks, lambda c: end_rows(c, inner).start())
+
+    @pl.when(is_mid)
+    def _():
+        x_spread(0).begin()
+
+    with scope("stage_wait2"):
+        for stage in after:
+            staged(stage)
+
+    def end_sends(what, stage, lo, hi):
+        @pl.when(is_end)
+        def _():
+            if what == "in":
+                each(lo, hi, lambda q: inward(stage, q, edge).start())
+            else:
+                each(lo, hi, lambda q: direct(stage, q).start())
+
+    end_sends("direct", first_vg, 0, shared_from)
+
+    @pl.when(is_mid)
+    def _():
+        for stage in after:
+            each(0, count[stage[1]], lambda q: outward(stage, q, mine).start())
+
+    gain_copy.wait()
+    for c in small:
+        c.wait()
+    for d in range(1, T):
+        pltpu.make_async_remote_copy(
+            src_ref=cgain.at[t], dst_ref=cgain.at[t], send_sem=g_sem.at[0], recv_sem=g_sem.at[1],
+            device_id={"tp": lax.rem(t + d, T)}, device_id_type=MESH).start()
+    x_state[...] = xg[0, t, own, :].astype(f32)
+    with scope("halo0_begin"):
+        halo(0, "begin")
+
+    def first_chunks(q):
+        from_inner(first_vg, q, near)
+        from_edge(first_vg, q)
+    with scope("A_vg0_near_edge"):
+        each(0, QC, first_chunks)
+    push_in(first_wo, 0, RC)
+    push_in(second_vg, 0, QC // 2)
+
+    @pl.when(is_end)
+    def _():
+        def pass_on(stage):
+            def body(q):
+                arrived(stage, q, mine)
+                across(stage, q, mine).start()
+            each(0, count[stage[1]], body)
+        for stage in after:
+            with scope("end_pass_on"):
+                pass_on(stage)
+            if stage == first_wo:
+                end_sends("in", first_wo, 0, RC)
+                end_sends("direct", first_wo, 0, RC)
+            elif stage == second_vg:
+                end_sends("in", second_vg, 0, QC // 2)
+
+    halo(0, "relay")
+    @pl.when(is_mid)
+    def _():
+        with scope("x0_finish"):
+            x_spread(0).relay()
+            x_spread(0).complete()
+    halo(0, "complete")
+
+    @pl.when(is_mid)
+    def _():
+        with scope("norm0"):
+            normalize(0, 0, 0, 0, full)
+
+    def second_chunks(q):
+        from_inner(first_vg, q, far)
+
+        @pl.when(is_mid)
+        def _():
+            wait_bytes(xg.at[0, t, pl.ds(0, x_rows)], f_sem.at[2 + q])
+            edge_spread(q).begin()
+
+            @pl.when(q > 0)
+            def _():
+                edge_spread(q - 1).relay()
+    with scope("B_vg0_far"):
+        each(0, QC, second_chunks)
+
+    @pl.when(is_mid)
+    def _():
+        with scope("edge_spread"):
+            edge_spread(x_chunks - 1).relay()
+            each(0, x_chunks - 1, lambda c: edge_spread(c).complete())
+    with scope("C1_wo0_near"):
+        from_inner(first_wo, 0, near)
+    end_sends("in", second_vg, QC // 2, QC)
+
+    @pl.when(is_mid)
+    def _():
+        with scope("edge_spread"):
+            edge_spread(x_chunks - 1).complete()
+        with scope("norm_e"):
+            normalize(0, L, 1, PAD, rows)
+
+    with scope("C1_wo0_near"):
+        each(1, RC, lambda q: from_inner(first_wo, q, near))
+
+    @pl.when(is_mid)
+    def _():
+        with scope("wait_vg0"):
+            others_arrived(first_vg)
+        with scope("proj0e"):
+            project(0, 1, PAD, rows, glu_out)
+
+    with scope("C2_wo0_edge"):
+        each(0, RC, lambda q: from_edge(first_wo, q))
+    push_in(second_vg, QC // 2, QC)
+    with scope("D1_vg1_near"):
+        from_inner(second_vg, 0, near)
+    end_sends("direct", second_vg, 0, QC // 2)
+
+    @pl.when(is_mid)
+    def _():
+        with scope("proj0"):
+            project(0, 0, 0, full, pad.at[0])
+
+    sends_right, sends_left, _, _ = sides_of(0)
+
+    @pl.when(sends_right)
+    def _():
+        glu_out[0:PAD, :] = jnp.zeros((PAD, chans), bf16)
+        glu_out[PAD + rows:, :] = pad[0, PAD:2 * PAD, :]
+        pad[0, 0:PAD, :] = glu_out[rows:rows + PAD, :]
+
+    @pl.when(sends_left)
+    def _():
+        glu_out[0:PAD, :] = pad[0, rows:rows + PAD, :]
+        glu_out[PAD + rows:, :] = jnp.zeros((PAD, chans), bf16)
+        pad[0, PAD + rows:, :] = glu_out[PAD:2 * PAD, :]
+
+    @pl.when(is_mid)
+    def _():
+        end_glu(edge).start()
+
+    with scope("C3_wo0_far"):
+        from_inner(first_wo, 0, far)
+
+    @pl.when(is_end)
+    def _():
+        with scope("end_glu_wait"):
+            wait_bytes(glu_out, f_sem.at[2 + x_chunks])
+    with scope("conv0"):
+        convolve(0)
+    with scope("C3_wo0_far"):
+        each(1, RC, lambda q: from_inner(first_wo, q, far))
+    with scope("D2_vg1_near"):
+        from_inner(second_vg, 1, near)
+    with scope("D2_vg1_edge"):
+        from_edge(second_vg, 0)
+    with scope("conv0_relay"):
+        conv_spread(0, 0).relay()
+        conv_spread(0, 1).relay()
+    with scope("D2_vg1_near"):
+        from_inner(second_vg, QC // 2, near)
+    with scope("conv0_complete"):
+        conv_spread(0, 0).complete()
+        conv_spread(0, 1).complete()
+        wait_bytes(cgain.at[pl.ds(0, T - 1)], g_sem.at[1])
+    with scope("wait_wo0"):
+        others_arrived(first_wo)
+    with scope("out0"):
+        add_branch(0)
+    xg[1, t, own, :] = x_state[...].astype(bf16)
+    x_spread(1).begin()
+    halo(1, "send")
+    end_sends("in", second_wo, 0, RC)
+    end_sends("direct", second_vg, QC // 2, QC)
+    end_sends("direct", second_wo, 0, RC)
+    with scope("D3_vg1_edge"):
+        each(1, QC // 2, lambda q: from_edge(second_vg, q))
+    with scope("D3_vg1_near"):
+        each(QC // 2 + 1, QC, lambda q: from_inner(second_vg, q, near))
+    with scope("D3_vg1_edge"):
+        each(QC // 2, QC, lambda q: from_edge(second_vg, q))
+    push_in(second_wo, 0, RC)
+    with scope("D4_vg1_far"):
+        each(0, QC // 2, lambda q: from_inner(second_vg, q, far))
+    with scope("halo1_begin"):
+        halo(1, "begin")
+    with scope("D4_vg1_far"):
+        each(QC // 2, QC, lambda q: from_inner(second_vg, q, far))
+    with scope("x1_relay"):
+        x_spread(1).relay()
+    with scope("E1_wo1_near"):
+        each(0, RC, lambda q: from_inner(second_wo, q, near))
+    with scope("halo1_relay"):
+        halo(1, "relay")
+    with scope("E1_wo1_edge"):
+        from_edge(second_wo, 0)
+    with scope("x1_complete"):
+        x_spread(1).complete()
+        halo(1, "complete")
+    with scope("norm1"):
+        normalize(1, 1, 0, 0, full)
+    with scope("E1_wo1_edge"):
+        each(1, RC, lambda q: from_edge(second_wo, q))
+    with scope("wait_vg1"):
+        others_arrived(second_vg)
+    with scope("proj1"):
+        project(1, 0, 0, full, pad.at[1])
+    with scope("E2_wo1_far"):
+        from_inner(second_wo, 0, far)
+    with scope("conv1"):
+        convolve(1)
+    with scope("E3_wo1_far"):
+        each(1, RC, lambda q: from_inner(second_wo, q, far))
+    with scope("conv1_gather"):
+        conv_spread(1, 0).relay()
+        conv_spread(1, 1).relay()
+        conv_spread(1, 0).complete()
+        conv_spread(1, 1).complete()
+    with scope("wait_wo1"):
+        others_arrived(second_wo)
+    with scope("out1"):
+        add_branch(1)
+    xf = x_state[...]
+    share(L, [jnp.sum(xf * xf, axis=1, keepdims=True)])
+
+    halo(0, "drain")
+    halo(1, "drain")
+    for layer in range(L):
+        for part_ in range(2):
+            conv_spread(layer, part_).drain()
+    x_spread(1).drain()
+    wait_bytes(cgain.at[pl.ds(0, T - 1)], g_sem.at[0])
+    chunk_rows = size["vg"]
+    stages = L * pieces
+    later = stages - QC
+
+    def sent(chunks, k):
+        wait_bytes(wvg.at[0, 0, pl.ds(0, chunks * chunk_rows)], send_w.at[k])
+
+    def sent_twice(chunks, k):
+        wait_bytes(wvg.at[0, :, pl.ds(0, chunks * chunk_rows)], send_w.at[k])
+
+    def sent_all(k):
+        sent_twice(later * (n - 1) // G, k)
+
+    @pl.when(is_mid)
+    def _():
+        x_spread(0).drain()
+        each(0, x_chunks, lambda c: edge_spread(c).drain())
+        wait_bytes(glu_out, f_sem.at[1])
+        sent_twice(stages, IN)
+        sent_all(OUT)
+        sent(QC - shared_from, YE)
+        sent_twice(later + QC, Y)
+
+    @pl.when(is_end)
+    def _():
+        wait_bytes(xg.at[0, t, own], f_sem.at[0])
+        sent(stages, IN)
+        sent(later + shared_from, UN)
+        sent_all(Y)
+
+    with scope("final_stat"):
+        got = columns_of(L)
+        for index_ in range(L + 1):
+            wait_bytes(stat.at[index_, pl.ds(0, T - 1)], s_sem.at[2 * index_])
+    total = sum((got[:, 8 * d:8 * d + 1] for d in range(1, T)), got[:, 0:1])
+    scale = lax.rsqrt(total / D + 1e-06)
+    result[...] = (x_state[...] * scale * fgain[...]).astype(bf16)
+
+
+def quad_on_device(G, n, T, tokens, norm_gain, value_w, gate_w, taps, cgain, out_w, fgain):
+    L = norm_gain.shape[0]
+    if L != 2:
+        return on_device(G, n, T, tokens, norm_gain, value_w, gate_w, taps, cgain, out_w, fgain)
+    rows, width = tokens.shape
+    depth, chans = value_w.shape[1:]
+    D, C = width * T, chans * T
+    bf16, f32 = jnp.bfloat16, jnp.float32
+    dma = pltpu.SemaphoreType.DMA
+    vmem = pl.BlockSpec(memory_space=pltpu.VMEM)
+    hbm = pl.BlockSpec(memory_space=pl.ANY)
+    full = rows + 2 * PAD
+    return pl.pallas_call(
+        functools.partial(quad_kernel, G, n, T, L),
+        out_shape=jax.ShapeDtypeStruct((rows, width), bf16),
+        in_specs=[hbm] * 8,
+        out_specs=vmem,
+        scratch_shapes=[
+            pltpu.VMEM((L, G, D, 2 * chans // G), bf16),
+            pltpu.VMEM((L, G, C, width // G), bf16),
+            pltpu.VMEM((L + 1, T, full, width), bf16),
+            pltpu.VMEM((2, T, full, width), bf16),
+            pltpu.VMEM((full, chans), bf16),
+            pltpu.VMEM((full, 2 * chans // G), f32),
+            pltpu.VMEM((L, full, chans), bf16),
+            pltpu.VMEM((full, chans), f32),
+            pltpu.VMEM((L, T, rows, chans), bf16),
+            pltpu.VMEM((L + 1, T, 8, rows), f32),
+            pltpu.VMEM((rows, width), f32),
+            pltpu.VMEM(norm_gain.shape, f32),
+            pltpu.VMEM((taps.shape[1], L, chans), f32),
+            pltpu.VMEM((T,) + cgain.shape, f32),
+            pltpu.VMEM((1, width), f32),
+            dma((2 * L + 5,)),
+            dma((L * (QC + RC), 3)), dma((2 * L,)), dma((5,)),
+            dma((L, 3)), dma((QC, 3)), dma((L, 2, 3)), dma((2 * (L + 1),)),
+            dma((L, 4)), dma((L, 2, 3)), dma((2,)), dma((QC + 3,)),
+        ],
+        compiler_params=pltpu.CompilerParams(
+            collective_id=0, has_side_effects=True, vmem_limit_bytes=56 * 2**20
+        ),
+    )(tokens, norm_gain, value_w, gate_w, taps.transpose(1, 0, 2), cgain, out_w, fgain.reshape(1, width))
 
 
 def tokens_f32(tokens, xg, t):
@@ -586,7 +1304,8 @@
         P("tp"),
     )
     G, n, T = (mesh.shape[a] for a in ("grp", "sp", "tp"))
+    paired = G == 2 and n == T == 2 * G
     return jax.shard_map(
-        functools.partial(on_device, G, n, T),
+        functools.partial(quad_on_device if paired else on_device, G, n, T),
         mesh=mesh, in_specs=placed, out_specs=P(("grp", "sp"), "tp"), check_vma=False,
     )

time: 127 us -> 103 us (0.81)
  Pallas kernels: 122 us -> 101 us
  local copies, waits for them, and re-layouts: 3.91 us -> 1.87 us
    pallas_call x1, Pallas kernels: 122 us -> 101 us  [quad_on_device(): pl.pallas_call(functools.partial(quad_kernel, G, n, T, L), out_shape=jax....]
    reshape x1 -> x0, local copies, waits for them, and re-layouts: 1.4 us -> none  [on_device(): norm_gain.reshape(L * T, width)]
where the time goes in v2:
time: 103 us
  Pallas kernels  101 us (98%)
  local copies, waits for them, and re-layouts  1.87 us (2%)
    pallas_call x1, Pallas kernels, quad_on_device(): pl.pallas_call(functools.partial(quad_kernel, G, n, T, L), out_shape=jax....  101 us

profile of v2, /device:TPU:0, one launch (start us, length us, event | category | flops | bytes accessed | tf_op | source)
XLA Modules:
  0.0 103.3 jit_solution(11780534322594263701)
XLA Ops:
  0.0 101.5 %shard_map.82 = bf16[256,1024]{1,0:T(8,128)(2,1)} custom-call(bf16[256,1024]{1,0:T(8,128)(2,1)} %tokens.1, f32[2,4096]{1,0:T(2,128)} %gain_hbm.1, bf16[2,1024,256]{2,1,0:T(8,128)(2,1)} %value_w.1, bf16[2,1024,256]{2,1,0:T(8,128)(2,1)} %gate_w.1, f32[31,2,256]{2,1,0:T(2,128)} %bitcast.2, f32[2,256]{1,0:T(2,128)} %cgain_hbm.1, bf16[2,256,1024]{2,1,0:T(8,128)(2,1)} %out_w.1, ...), custom_call_target="tpu_custom_call" | custom-call | tf_op jit(solution)/shard_map/pallas_call | solution.py:1216
  101.5 1.9 %copy.10 = bf16[256,1024]{1,0:T(8,128)(2,1)} copy(bf16[256,1024]{1,0:T(8,128)(2,1)} %shard_map.82) | data formatting | bytes 1048576

commit v3 on v2

--- a/solution.py
+++ b/solution.py
@@ -535,7 +535,7 @@
     G, n, T, L,
     tokens, gain_hbm, value_w, gate_w, taps_hbm, cgain_hbm, out_w, fgain_hbm,
     result,
-    wvg, wo, xg, xn, glu_out, acc, pad, padf, convg, stat, x_state, gain, taps, cgain, fgain,
+    wvg, wo, xg, xn, glu_out, acc, pad, padf, convg, act, stat, x_state, gain, taps, cgain, fgain,
     local_sem, recv_z, recv_o, send_w, x_sem, e_sem, c_sem, s_sem, h_sem, hs_sem, g_sem, f_sem,
 ):
     g, s, t = lax.axis_index("grp"), lax.axis_index("sp"), lax.axis_index("tp")
@@ -712,14 +712,16 @@
             return carry
         lax.fori_loop(low_, high_, step, 0)
 
-    def from_inner(stage, q, j):
+    def from_inner(stage, q, j, over_y=True):
         def serve():
-            arrived(stage, q, j)
+            with scope("w_inner"):
+                arrived(stage, q, j)
             if stage != first_vg:
                 @pl.when(is_mid)
                 def _():
                     outward(stage, q, j).start()
-            across(stage, q, j).start()
+            if over_y:
+                across(stage, q, j).start()
         if stage == first_vg:
             pl.when(is_mid)(serve)
         else:
@@ -728,7 +730,8 @@
     def from_edge(stage, q):
         @pl.when(is_mid)
         def _():
-            arrived(stage, q, edge)
+            with scope("w_edge"):
+                arrived(stage, q, edge)
             inward(stage, q, edge).start()
             if stage == first_vg:
                 @pl.when(q >= shared_from)
@@ -764,9 +767,17 @@
         def drain(self):
             wait_bytes(self.three, self.sems(2))
 
-    def x_spread(layer):
-        return Spread(lambda j: xg.at[layer, j, own], xg.at[layer, pl.ds(0, 3), own], xg.at[layer, pl.ds(0, 2), own],
-                      lambda k: x_sem.at[layer, k])
+    def half_columns(h):
+        return pl.ds(pl.multiple_of(h * out_half, out_half), out_half)
+
+    def x_spread():
+        return Spread(lambda j: xg.at[0, j, own], xg.at[0, pl.ds(0, 3), own], xg.at[0, pl.ds(0, 2), own],
+                      lambda k: x_sem.at[0, k])
+
+    def half_spread(h, turn):
+        cols = half_columns(h)
+        return Spread(lambda j: xg.at[1, j, own, cols], xg.at[1, pl.ds(0, 3), own, cols],
+                      xg.at[1, pl.ds(0, 2), own, cols], lambda k: x_sem.at[1 + turn, k])
 
     def edge_spread(c):
         part = pl.ds(pl.multiple_of(PAD + c * x_rows, PAD), x_rows)
@@ -816,23 +827,22 @@
             return carry
         lax.fori_loop(0, T, body, 0)
 
-    def project(layer, held, start, size_, into):
-        for h in range(G):
-            def body(j, carry):
-                block = wvg[layer, h, pl.ds(pl.multiple_of(j * width, width), width), :]
-                part = jnp.dot(xn[held, j, start:start + size_, :], block, preferred_element_type=f32)
-
-                @pl.when(j == 0)
-                def _():
-                    acc[start:start + size_, :] = part
-
-                @pl.when(j > 0)
-                def _():
-                    acc[start:start + size_, :] += part
-                return carry
-            lax.fori_loop(0, T, body, 0)
-            glu = acc[start:start + size_, :half] * jax.nn.sigmoid(acc[start:start + size_, half:])
-            into[start:start + size_, h * half:(h + 1) * half] = glu.astype(bf16)
+    def project(layer, held, start, size_, into, h):
+        def body(j, carry):
+            block = wvg[layer, h, pl.ds(pl.multiple_of(j * width, width), width), :]
+            part = jnp.dot(xn[held, j, start:start + size_, :], block, preferred_element_type=f32)
+
+            @pl.when(j == 0)
+            def _():
+                acc[start:start + size_, :] = part
+
+            @pl.when(j > 0)
+            def _():
+                acc[start:start + size_, :] += part
+            return carry
+        lax.fori_loop(0, T, body, 0)
+        glu = acc[start:start + size_, :half] * jax.nn.sigmoid(acc[start:start + size_, half:])
+        into[start:start + size_, pl.ds(pl.multiple_of(h * half, half), half)] = glu.astype(bf16)
 
     def x_right(layer):
         return pltpu.make_async_remote_copy(
@@ -880,7 +890,7 @@
             pl.when(from_left)(lambda: getattr(halo_spread(layer, 0), do)())
             pl.when(from_right)(lambda: getattr(halo_spread(layer, 1), do)())
 
-    def convolve(layer):
+    def convolve(layer, between):
         padf[...] = pad[layer].astype(f32)
         block = 64
         sums, squares = [], []
@@ -896,29 +906,30 @@
             squares.append(jnp.sum(shifted * shifted, axis=1, keepdims=True))
             if r + block == rows // 2:
                 conv_spread(layer, 0).begin()
+                between()
         share(layer, [jnp.concatenate(sums, 0), jnp.concatenate(squares, 0)])
         conv_spread(layer, 1).begin()
 
-    def add_branch(layer):
+    def activate(layer):
         got = columns_of(layer)
         means = [got[:, 8 * d:8 * d + 1] for d in range(T)]
         center = sum(means[1:], means[0]) / T
         apart = [m - center for m in means]
         square = sum((got[:, 8 * d + 1:8 * d + 2] + chans * (apart[d] * apart[d]) for d in range(T)), jnp.zeros((rows, 1), f32))
         scale = lax.rsqrt(square / C + 1e-05)
-        parts = [None] * G
         for d in range(T):
             j = lax.rem(t + T - d, T)
             by = cgain[j, layer:layer + 1, :]
             normal = (convg[layer, j].astype(f32) + apart[d]) * scale
-            act = jax.nn.silu(normal * by).astype(bf16)
-            for h in range(G):
-                block = wo[layer, h, pl.ds(pl.multiple_of(j * chans, chans), chans), :]
-                term = jnp.dot(act, block, preferred_element_type=f32)
-                parts[h] = term if parts[h] is None else parts[h] + term
-        for h in range(G):
-            cols = slice(h * out_half, (h + 1) * out_half)
-            x_state[:, cols] = (x_state[:, cols] + parts[h]).astype(bf16).astype(f32)
+            act[j] = jax.nn.silu(normal * by).astype(bf16)
+
+    def add_branch(layer, h):
+        part = None
+        for j in range(T):
+            term = jnp.dot(act[j], wo[layer, h, j * chans:(j + 1) * chans, :], preferred_element_type=f32)
+            part = term if part is None else part + term
+        cols = half_columns(h)
+        x_state[:, cols] = (x_state[:, cols] + part).astype(bf16).astype(f32)
 
     with scope("stage_wait"):
         staged(first_vg)
@@ -932,7 +943,7 @@
 
     @pl.when(is_mid)
     def _():
-        x_spread(0).begin()
+        x_spread().begin()
 
     with scope("stage_wait2"):
         for stage in after:
@@ -984,16 +995,23 @@
                 pass_on(stage)
             if stage == first_wo:
                 end_sends("in", first_wo, 0, RC)
+                end_sends("in", second_vg, 0, QC // 2)
+            elif stage == second_vg:
                 end_sends("direct", first_wo, 0, RC)
-            elif stage == second_vg:
-                end_sends("in", second_vg, 0, QC // 2)
+
+    def edge_relays(lo, hi):
+        @pl.when(is_mid)
+        def _():
+            with scope("edge_relay"):
+                each(lo, hi, lambda c: edge_spread(c).relay())
 
     halo(0, "relay")
+
     @pl.when(is_mid)
     def _():
         with scope("x0_finish"):
-            x_spread(0).relay()
-            x_spread(0).complete()
+            x_spread().relay()
+            x_spread().complete()
     halo(0, "complete")
 
     @pl.when(is_mid)
@@ -1008,50 +1026,48 @@
         def _():
             wait_bytes(xg.at[0, t, pl.ds(0, x_rows)], f_sem.at[2 + q])
             edge_spread(q).begin()
-
-            @pl.when(q > 0)
-            def _():
-                edge_spread(q - 1).relay()
     with scope("B_vg0_far"):
         each(0, QC, second_chunks)
 
     @pl.when(is_mid)
     def _():
-        with scope("edge_spread"):
-            edge_spread(x_chunks - 1).relay()
-            each(0, x_chunks - 1, lambda c: edge_spread(c).complete())
+        with scope("proj0_g"):
+            project(0, 0, 0, full, pad.at[0], g)
+    edge_relays(0, x_chunks // 2)
     with scope("C1_wo0_near"):
         from_inner(first_wo, 0, near)
+    edge_relays(x_chunks // 2, x_chunks - 1)
+    with scope("C1_wo0_near"):
+        each(1, RC, lambda q: from_inner(first_wo, q, near))
+    edge_relays(x_chunks - 1, x_chunks)
+    push_in(second_vg, QC // 2, QC // 2 + 1)
     end_sends("in", second_vg, QC // 2, QC)
 
     @pl.when(is_mid)
     def _():
-        with scope("edge_spread"):
-            edge_spread(x_chunks - 1).complete()
+        with scope("edge_complete"):
+            each(0, x_chunks, lambda c: edge_spread(c).complete())
         with scope("norm_e"):
             normalize(0, L, 1, PAD, rows)
-
-    with scope("C1_wo0_near"):
-        each(1, RC, lambda q: from_inner(first_wo, q, near))
+        with scope("proj0e_g"):
+            project(0, 1, PAD, rows, glu_out, g)
+
+    with scope("D1_vg1_near"):
+        from_inner(second_vg, 0, near)
 
     @pl.when(is_mid)
     def _():
         with scope("wait_vg0"):
             others_arrived(first_vg)
         with scope("proj0e"):
-            project(0, 1, PAD, rows, glu_out)
-
+            project(0, 1, PAD, rows, glu_out, other)
     with scope("C2_wo0_edge"):
-        each(0, RC, lambda q: from_edge(first_wo, q))
-    push_in(second_vg, QC // 2, QC)
-    with scope("D1_vg1_near"):
-        from_inner(second_vg, 0, near)
-    end_sends("direct", second_vg, 0, QC // 2)
+        from_edge(first_wo, 0)
 
     @pl.when(is_mid)
     def _():
         with scope("proj0"):
-            project(0, 0, 0, full, pad.at[0])
+            project(0, 0, 0, full, pad.at[0], other)
 
     sends_right, sends_left, _, _ = sides_of(0)
 
@@ -1071,87 +1087,120 @@
     def _():
         end_glu(edge).start()
 
+    with scope("D1_vg1_near"):
+        each(1, QC // 2, lambda q: from_inner(second_vg, q, near))
+    with scope("C2_wo0_edge"):
+        each(1, RC, lambda q: from_edge(first_wo, q))
+    push_in(second_vg, QC // 2 + 1, QC)
+    end_sends("in", second_wo, 0, RC)
+
+    @pl.when(is_end)
+    def _():
+        with scope("end_glu_wait"):
+            wait_bytes(glu_out, f_sem.at[2 + x_chunks])
+
+    with scope("conv0"):
+        convolve(0, lambda: None)
+    with scope("D2_vg1_edge"):
+        from_edge(second_vg, 0)
     with scope("C3_wo0_far"):
         from_inner(first_wo, 0, far)
-
-    @pl.when(is_end)
-    def _():
-        with scope("end_glu_wait"):
-            wait_bytes(glu_out, f_sem.at[2 + x_chunks])
-    with scope("conv0"):
-        convolve(0)
-    with scope("C3_wo0_far"):
-        each(1, RC, lambda q: from_inner(first_wo, q, far))
-    with scope("D2_vg1_near"):
-        from_inner(second_vg, 1, near)
-    with scope("D2_vg1_edge"):
-        from_edge(second_vg, 0)
     with scope("conv0_relay"):
         conv_spread(0, 0).relay()
+    with scope("C3_wo0_far"):
+        pl.when(is_end)(lambda: each(1, RC, lambda q: from_inner(first_wo, q, far)))
+    with scope("conv0_relay"):
         conv_spread(0, 1).relay()
-    with scope("D2_vg1_near"):
-        from_inner(second_vg, QC // 2, near)
+    with scope("C3_wo0_far"):
+        pl.when(is_mid)(lambda: each(1, RC, lambda q: from_inner(first_wo, q, far)))
     with scope("conv0_complete"):
         conv_spread(0, 0).complete()
         conv_spread(0, 1).complete()
         wait_bytes(cgain.at[pl.ds(0, T - 1)], g_sem.at[1])
+    with scope("act0"):
+        activate(0)
+    with scope("D2_vg1_edge"):
+        from_edge(second_vg, 1)
+
+    def next_x(h, turn):
+        add_branch(0, h)
+        cols = half_columns(h)
+        xg[1, t, own, cols] = x_state[:, cols].astype(bf16)
+        half_spread(h, turn).begin()
+    with scope("out0_g"):
+        next_x(g, 0)
+    with scope("D2_vg1_near"):
+        from_inner(second_vg, QC // 2, near)
     with scope("wait_wo0"):
         others_arrived(first_wo)
     with scope("out0"):
-        add_branch(0)
-    xg[1, t, own, :] = x_state[...].astype(bf16)
-    x_spread(1).begin()
+        next_x(other, 1)
     halo(1, "send")
-    end_sends("in", second_wo, 0, RC)
-    end_sends("direct", second_vg, QC // 2, QC)
+    end_sends("direct", second_vg, 0, QC)
     end_sends("direct", second_wo, 0, RC)
-    with scope("D3_vg1_edge"):
-        each(1, QC // 2, lambda q: from_edge(second_vg, q))
     with scope("D3_vg1_near"):
         each(QC // 2 + 1, QC, lambda q: from_inner(second_vg, q, near))
     with scope("D3_vg1_edge"):
-        each(QC // 2, QC, lambda q: from_edge(second_vg, q))
+        from_edge(second_vg, 2)
+    with scope("D4_vg1_far"):
+        from_inner(second_vg, 0, far)
+    with scope("D3_vg1_edge"):
+        each(3, QC, lambda q: from_edge(second_vg, q))
     push_in(second_wo, 0, RC)
     with scope("D4_vg1_far"):
-        each(0, QC // 2, lambda q: from_inner(second_vg, q, far))
+        from_inner(second_vg, 1, far)
+    with scope("x1_relay"):
+        half_spread(g, 0).relay()
+    with scope("D4_vg1_far"):
+        from_inner(second_vg, 2, far)
+    with scope("E1_wo1_edge"):
+        from_edge(second_wo, 0)
+    with scope("D4_vg1_far"):
+        each(3, QC, lambda q: from_inner(second_vg, q, far))
+    with scope("E1_wo1_edge"):
+        each(1, RC, lambda q: from_edge(second_wo, q))
     with scope("halo1_begin"):
         halo(1, "begin")
-    with scope("D4_vg1_far"):
-        each(QC // 2, QC, lambda q: from_inner(second_vg, q, far))
     with scope("x1_relay"):
-        x_spread(1).relay()
+        half_spread(other, 1).relay()
     with scope("E1_wo1_near"):
-        each(0, RC, lambda q: from_inner(second_wo, q, near))
+        from_inner(second_wo, 0, near)
     with scope("halo1_relay"):
         halo(1, "relay")
-    with scope("E1_wo1_edge"):
-        from_edge(second_wo, 0)
     with scope("x1_complete"):
-        x_spread(1).complete()
+        half_spread(g, 0).complete()
+        half_spread(other, 1).complete()
         halo(1, "complete")
     with scope("norm1"):
         normalize(1, 1, 0, 0, full)
-    with scope("E1_wo1_edge"):
-        each(1, RC, lambda q: from_edge(second_wo, q))
+    with scope("E1_wo1_near"):
+        each(1, RC, lambda q: from_inner(second_wo, q, near))
+    with scope("proj1_g"):
+        project(1, 0, 0, full, pad.at[1], g)
+    with scope("E2_wo1_far_m"):
+        pl.when(is_mid)(lambda: from_inner(second_wo, 0, far))
     with scope("wait_vg1"):
         others_arrived(second_vg)
     with scope("proj1"):
-        project(1, 0, 0, full, pad.at[1])
-    with scope("E2_wo1_far"):
-        from_inner(second_wo, 0, far)
+        project(1, 0, 0, full, pad.at[1], other)
+    with scope("E2_wo1_far_e"):
+        pl.when(is_end)(lambda: from_inner(second_wo, 0, far))
     with scope("conv1"):
-        convolve(1)
-    with scope("E3_wo1_far"):
-        each(1, RC, lambda q: from_inner(second_wo, q, far))
+        convolve(1, lambda: pl.when(is_mid)(lambda: each(1, RC, lambda q: from_inner(second_wo, q, far))))
     with scope("conv1_gather"):
         conv_spread(1, 0).relay()
+        pl.when(is_end)(lambda: each(1, RC, lambda q: from_inner(second_wo, q, far)))
         conv_spread(1, 1).relay()
         conv_spread(1, 0).complete()
         conv_spread(1, 1).complete()
+    with scope("act1"):
+        activate(1)
+    with scope("out1_g"):
+        add_branch(1, g)
     with scope("wait_wo1"):
         others_arrived(second_wo)
     with scope("out1"):
-        add_branch(1)
+        add_branch(1, other)
     xf = x_state[...]
     share(L, [jnp.sum(xf * xf, axis=1, keepdims=True)])
 
@@ -1160,7 +1209,8 @@
     for layer in range(L):
         for part_ in range(2):
             conv_spread(layer, part_).drain()
-    x_spread(1).drain()
+    half_spread(g, 0).drain()
+    half_spread(other, 1).drain()
     wait_bytes(cgain.at[pl.ds(0, T - 1)], g_sem.at[0])
     chunk_rows = size["vg"]
     stages = L * pieces
@@ -1177,7 +1227,7 @@
 
     @pl.when(is_mid)
     def _():
-        x_spread(0).drain()
+        x_spread().drain()
         each(0, x_chunks, lambda c: edge_spread(c).drain())
         wait_bytes(glu_out, f_sem.at[1])
         sent_twice(stages, IN)
@@ -1228,6 +1278,7 @@
             pltpu.VMEM((L, full, chans), bf16),
             pltpu.VMEM((full, chans), f32),
             pltpu.VMEM((L, T, rows, chans), bf16),
+            pltpu.VMEM((T, rows, chans), bf16),
             pltpu.VMEM((L + 1, T, 8, rows), f32),
             pltpu.VMEM((rows, width), f32),
             pltpu.VMEM(norm_gain.shape, f32),
@@ -1236,7 +1287,7 @@
             pltpu.VMEM((1, width), f32),
             dma((2 * L + 5,)),
             dma((L * (QC + RC), 3)), dma((2 * L,)), dma((5,)),
-            dma((L, 3)), dma((QC, 3)), dma((L, 2, 3)), dma((2 * (L + 1),)),
+            dma((1 + G, 3)), dma((QC, 3)), dma((L, 2, 3)), dma((2 * (L + 1),)),
             dma((L, 4)), dma((L, 2, 3)), dma((2,)), dma((QC + 3,)),
         ],
         compiler_params=pltpu.CompilerParams(

time: 103 us -> 98.7 us (0.958)
  Pallas kernels: 101 us -> 96.6 us
    pallas_call x1, Pallas kernels: 101 us -> 96.6 us  [quad_on_device(): pl.pallas_call(functools.partial(quad_kernel, G, n, T, L), out_shape=jax....]
where the time goes in v3:
time: 98.7 us; the launch traced here: 98.5 us
  Pallas kernels  96.6 us (98%)
  local copies, waits for them, and re-layouts  1.87 us (2%)
    pallas_call x1, Pallas kernels, quad_on_device(): pl.pallas_call(functools.partial(quad_kernel, G, n, T, L), out_shape=jax....  96.6 us

profile of v3, /device:TPU:0, one launch (start us, length us, event | category | flops | bytes accessed | tf_op | source)
XLA Modules:
  0.0 98.5 jit_solution(8815655935489535129)
XLA Ops:
  0.0 96.6 %shard_map.82 = bf16[256,1024]{1,0:T(8,128)(2,1)} custom-call(bf16[256,1024]{1,0:T(8,128)(2,1)} %tokens.1, f32[2,4096]{1,0:T(2,128)} %gain_hbm.1, bf16[2,1024,256]{2,1,0:T(8,128)(2,1)} %value_w.1, bf16[2,1024,256]{2,1,0:T(8,128)(2,1)} %gate_w.1, f32[31,2,256]{2,1,0:T(2,128)} %bitcast.2, f32[2,256]{1,0:T(2,128)} %cgain_hbm.1, bf16[2,256,1024]{2,1,0:T(8,128)(2,1)} %out_w.1, ...), custom_call_target="tpu_custom_call" | custom-call | tf_op jit(solution)/shard_map/pallas_call | solution.py:1266
  96.6 1.9 %copy.10 = bf16[256,1024]{1,0:T(8,128)(2,1)} copy(bf16[256,1024]{1,0:T(8,128)(2,1)} %shard_map.82) | data formatting | bytes 1048576

commit v4 on v3

--- a/solution.py
+++ b/solution.py
@@ -528,15 +528,16 @@
 
 
 QC = 4
-RC = 2
+RC = 4
+EPILOGUE = 2
 
 
 def quad_kernel(
     G, n, T, L,
-    tokens, gain_hbm, value_w, gate_w, taps_hbm, cgain_hbm, out_w, fgain_hbm,
-    result,
-    wvg, wo, xg, xn, glu_out, acc, pad, padf, convg, act, stat, x_state, gain, taps, cgain, fgain,
-    local_sem, recv_z, recv_o, send_w, x_sem, e_sem, c_sem, s_sem, h_sem, hs_sem, g_sem, f_sem,
+    tokens, gain_hbm, value_w, gate_w, taps_hbm, cgain_hbm, out_w,
+    x_out, scale_out,
+    wvg, wo, xg, xn, glu_out, acc, pad, padf, convg, act, stat, x_state, leaving, gain, taps, cgain,
+    local_sem, recv_z, recv_o, send_w, x_sem, e_sem, c_sem, s_sem, h_sem, hs_sem, g_sem, f_sem, o_sem,
 ):
     g, s, t = lax.axis_index("grp"), lax.axis_index("sp"), lax.axis_index("tp")
     rows, width = tokens.shape
@@ -617,7 +618,6 @@
     small = [
         pltpu.make_async_copy(gain_hbm, gain, local_sem.at[2 * L + 2]),
         pltpu.make_async_copy(taps_hbm, taps, local_sem.at[2 * L + 3]),
-        pltpu.make_async_copy(fgain_hbm, fgain, local_sem.at[2 * L + 4]),
     ]
     stage_in(first_vg)
     token_copy.start()
@@ -1035,10 +1035,10 @@
             project(0, 0, 0, full, pad.at[0], g)
     edge_relays(0, x_chunks // 2)
     with scope("C1_wo0_near"):
-        from_inner(first_wo, 0, near)
+        each(0, RC // 2, lambda q: from_inner(first_wo, q, near))
     edge_relays(x_chunks // 2, x_chunks - 1)
     with scope("C1_wo0_near"):
-        each(1, RC, lambda q: from_inner(first_wo, q, near))
+        each(RC // 2, RC, lambda q: from_inner(first_wo, q, near))
     edge_relays(x_chunks - 1, x_chunks)
     push_in(second_vg, QC // 2, QC // 2 + 1)
     end_sends("in", second_vg, QC // 2, QC)
@@ -1062,7 +1062,7 @@
         with scope("proj0e"):
             project(0, 1, PAD, rows, glu_out, other)
     with scope("C2_wo0_edge"):
-        from_edge(first_wo, 0)
+        each(0, RC // 2, lambda q: from_edge(first_wo, q))
 
     @pl.when(is_mid)
     def _():
@@ -1090,7 +1090,7 @@
     with scope("D1_vg1_near"):
         each(1, QC // 2, lambda q: from_inner(second_vg, q, near))
     with scope("C2_wo0_edge"):
-        each(1, RC, lambda q: from_edge(first_wo, q))
+        each(RC // 2, RC, lambda q: from_edge(first_wo, q))
     push_in(second_vg, QC // 2 + 1, QC)
     end_sends("in", second_wo, 0, RC)
 
@@ -1104,15 +1104,15 @@
     with scope("D2_vg1_edge"):
         from_edge(second_vg, 0)
     with scope("C3_wo0_far"):
-        from_inner(first_wo, 0, far)
+        each(0, RC // 2, lambda q: from_inner(first_wo, q, far))
     with scope("conv0_relay"):
         conv_spread(0, 0).relay()
     with scope("C3_wo0_far"):
-        pl.when(is_end)(lambda: each(1, RC, lambda q: from_inner(first_wo, q, far)))
+        pl.when(is_end)(lambda: each(RC // 2, RC, lambda q: from_inner(first_wo, q, far)))
     with scope("conv0_relay"):
         conv_spread(0, 1).relay()
     with scope("C3_wo0_far"):
-        pl.when(is_mid)(lambda: each(1, RC, lambda q: from_inner(first_wo, q, far)))
+        pl.when(is_mid)(lambda: each(RC // 2, RC, lambda q: from_inner(first_wo, q, far)))
     with scope("conv0_complete"):
         conv_spread(0, 0).complete()
         conv_spread(0, 1).complete()
@@ -1121,6 +1121,7 @@
         activate(0)
     with scope("D2_vg1_edge"):
         from_edge(second_vg, 1)
+    push_in(second_wo, 0, RC // 2)
 
     def next_x(h, turn):
         add_branch(0, h)
@@ -1146,27 +1147,33 @@
         from_inner(second_vg, 0, far)
     with scope("D3_vg1_edge"):
         each(3, QC, lambda q: from_edge(second_vg, q))
-    push_in(second_wo, 0, RC)
+    push_in(second_wo, RC // 2, RC)
     with scope("D4_vg1_far"):
         from_inner(second_vg, 1, far)
     with scope("x1_relay"):
         half_spread(g, 0).relay()
+    with scope("halo1_begin"):
+        pl.when(is_end)(lambda: halo(1, "begin"))
     with scope("D4_vg1_far"):
         from_inner(second_vg, 2, far)
+    with scope("x1_relay"):
+        pl.when(is_end)(half_spread(other, 1).relay)
+    with scope("halo1_relay"):
+        pl.when(is_end)(lambda: halo(1, "relay"))
     with scope("E1_wo1_edge"):
-        from_edge(second_wo, 0)
+        each(0, RC // 2, lambda q: from_edge(second_wo, q))
     with scope("D4_vg1_far"):
         each(3, QC, lambda q: from_inner(second_vg, q, far))
     with scope("E1_wo1_edge"):
-        each(1, RC, lambda q: from_edge(second_wo, q))
+        each(RC // 2, RC, lambda q: from_edge(second_wo, q))
     with scope("halo1_begin"):
-        halo(1, "begin")
+        pl.when(is_mid)(lambda: halo(1, "begin"))
     with scope("x1_relay"):
-        half_spread(other, 1).relay()
+        pl.when(is_mid)(half_spread(other, 1).relay)
     with scope("E1_wo1_near"):
-        from_inner(second_wo, 0, near)
+        pl.when(is_mid)(lambda: each(0, RC // 2, lambda q: from_inner(second_wo, q, near)))
     with scope("halo1_relay"):
-        halo(1, "relay")
+        pl.when(is_mid)(lambda: halo(1, "relay"))
     with scope("x1_complete"):
         half_spread(g, 0).complete()
         half_spread(other, 1).complete()
@@ -1174,33 +1181,48 @@
     with scope("norm1"):
         normalize(1, 1, 0, 0, full)
     with scope("E1_wo1_near"):
-        each(1, RC, lambda q: from_inner(second_wo, q, near))
+        pl.when(is_mid)(lambda: each(RC // 2, RC, lambda q: from_inner(second_wo, q, near)))
     with scope("proj1_g"):
         project(1, 0, 0, full, pad.at[1], g)
-    with scope("E2_wo1_far_m"):
-        pl.when(is_mid)(lambda: from_inner(second_wo, 0, far))
+    with scope("E2_m"):
+        pl.when(is_mid)(lambda: each(0, RC // 2, lambda q: from_inner(second_wo, q, far)))
+    with scope("E1_e"):
+        pl.when(is_end)(lambda: each(0, RC // 2, lambda q: from_inner(second_wo, q, near)))
     with scope("wait_vg1"):
         others_arrived(second_vg)
     with scope("proj1"):
         project(1, 0, 0, full, pad.at[1], other)
-    with scope("E2_wo1_far_e"):
-        pl.when(is_end)(lambda: from_inner(second_wo, 0, far))
+    with scope("E1_e"):
+        pl.when(is_end)(lambda: each(RC // 2, RC, lambda q: from_inner(second_wo, q, near)))
+    with scope("E2_m"):
+        pl.when(is_mid)(lambda: each(RC // 2, RC, lambda q: from_inner(second_wo, q, far)))
     with scope("conv1"):
-        convolve(1, lambda: pl.when(is_mid)(lambda: each(1, RC, lambda q: from_inner(second_wo, q, far))))
+        convolve(1, lambda: None)
+    with scope("E2_e"):
+        pl.when(is_end)(lambda: each(0, RC // 2, lambda q: from_inner(second_wo, q, far)))
+    with scope("conv1_relay"):
+        conv_spread(1, 0).relay()
+    with scope("E2_e"):
+        pl.when(is_end)(lambda: each(RC // 2, RC, lambda q: from_inner(second_wo, q, far)))
+    with scope("conv1_relay"):
+        conv_spread(1, 1).relay()
     with scope("conv1_gather"):
-        conv_spread(1, 0).relay()
-        pl.when(is_end)(lambda: each(1, RC, lambda q: from_inner(second_wo, q, far)))
-        conv_spread(1, 1).relay()
         conv_spread(1, 0).complete()
         conv_spread(1, 1).complete()
     with scope("act1"):
         activate(1)
+
+    def last_x(h, turn):
+        add_branch(1, h)
+        cols = half_columns(h)
+        leaving[:, cols] = x_state[:, cols].astype(bf16)
+        pltpu.make_async_copy(leaving.at[:, cols], x_out.at[:, cols], o_sem.at[turn]).start()
     with scope("out1_g"):
-        add_branch(1, g)
+        last_x(g, 0)
     with scope("wait_wo1"):
         others_arrived(second_wo)
     with scope("out1"):
-        add_branch(1, other)
+        last_x(other, 1)
     xf = x_state[...]
     share(L, [jnp.sum(xf * xf, axis=1, keepdims=True)])
 
@@ -1212,15 +1234,14 @@
     half_spread(g, 0).drain()
     half_spread(other, 1).drain()
     wait_bytes(cgain.at[pl.ds(0, T - 1)], g_sem.at[0])
-    chunk_rows = size["vg"]
-    stages = L * pieces
-    later = stages - QC
-
-    def sent(chunks, k):
-        wait_bytes(wvg.at[0, 0, pl.ds(0, chunks * chunk_rows)], send_w.at[k])
-
-    def sent_twice(chunks, k):
-        wait_bytes(wvg.at[0, :, pl.ds(0, chunks * chunk_rows)], send_w.at[k])
+    whole = L * (depth + out_rows * out_half // (2 * half))
+    later = whole - depth
+
+    def sent(length, k):
+        wait_bytes(wvg.at[0, 0, pl.ds(0, length)], send_w.at[k])
+
+    def sent_twice(length, k):
+        wait_bytes(wvg.at[0, :, pl.ds(0, length)], send_w.at[k])
 
     def sent_all(k):
         sent_twice(later * (n - 1) // G, k)
@@ -1230,25 +1251,30 @@
         x_spread().drain()
         each(0, x_chunks, lambda c: edge_spread(c).drain())
         wait_bytes(glu_out, f_sem.at[1])
-        sent_twice(stages, IN)
-        sent_all(OUT)
-        sent(QC - shared_from, YE)
-        sent_twice(later + QC, Y)
+        sent_twice(whole, IN)
+        sent_twice(3 * later // 2, OUT)
+        sent((QC - shared_from) * size["vg"], YE)
+        sent_twice(whole, Y)
 
     @pl.when(is_end)
     def _():
         wait_bytes(xg.at[0, t, own], f_sem.at[0])
-        sent(stages, IN)
-        sent(later + shared_from, UN)
-        sent_all(Y)
+        sent(whole, IN)
+        sent(later + shared_from * size["vg"], UN)
+        sent_twice(3 * later // 2, Y)
 
     with scope("final_stat"):
         got = columns_of(L)
         for index_ in range(L + 1):
             wait_bytes(stat.at[index_, pl.ds(0, T - 1)], s_sem.at[2 * index_])
     total = sum((got[:, 8 * d:8 * d + 1] for d in range(1, T)), got[:, 0:1])
-    scale = lax.rsqrt(total / D + 1e-06)
-    result[...] = (x_state[...] * scale * fgain[...]).astype(bf16)
+    scale_out[...] = lax.rsqrt(total / D + 1e-06)
+    for turn in range(G):
+        wait_bytes(leaving.at[:, pl.ds(0, out_half)], o_sem.at[turn])
+
+
+def scale_rows(x, scale, gain, out):
+    out[...] = (x[...].astype(jnp.float32) * scale[...] * gain[...]).astype(out.dtype)
 
 
 def quad_on_device(G, n, T, tokens, norm_gain, value_w, gate_w, taps, cgain, out_w, fgain):
@@ -1261,13 +1287,13 @@
     bf16, f32 = jnp.bfloat16, jnp.float32
     dma = pltpu.SemaphoreType.DMA
     vmem = pl.BlockSpec(memory_space=pltpu.VMEM)
-    hbm = pl.BlockSpec(memory_space=pl.ANY)
+    hbm = pl.BlockSpec(memory_space=pltpu.HBM)
     full = rows + 2 * PAD
-    return pl.pallas_call(
+    x, scale = pl.pallas_call(
         functools.partial(quad_kernel, G, n, T, L),
-        out_shape=jax.ShapeDtypeStruct((rows, width), bf16),
-        in_specs=[hbm] * 8,
-        out_specs=vmem,
+        out_shape=(jax.ShapeDtypeStruct((rows, width), bf16), jax.ShapeDtypeStruct((rows, 1), f32)),
+        in_specs=[hbm] * 7,
+        out_specs=(pl.BlockSpec(memory_space=pl.ANY), vmem),
         scratch_shapes=[
             pltpu.VMEM((L, G, D, 2 * chans // G), bf16),
             pltpu.VMEM((L, G, C, width // G), bf16),
@@ -1281,19 +1307,32 @@
             pltpu.VMEM((T, rows, chans), bf16),
             pltpu.VMEM((L + 1, T, 8, rows), f32),
             pltpu.VMEM((rows, width), f32),
+            pltpu.VMEM((rows, width), bf16),
             pltpu.VMEM(norm_gain.shape, f32),
             pltpu.VMEM((taps.shape[1], L, chans), f32),
             pltpu.VMEM((T,) + cgain.shape, f32),
-            pltpu.VMEM((1, width), f32),
-            dma((2 * L + 5,)),
+            dma((2 * L + 4,)),
             dma((L * (QC + RC), 3)), dma((2 * L,)), dma((5,)),
             dma((1 + G, 3)), dma((QC, 3)), dma((L, 2, 3)), dma((2 * (L + 1),)),
-            dma((L, 4)), dma((L, 2, 3)), dma((2,)), dma((QC + 3,)),
+            dma((L, 4)), dma((L, 2, 3)), dma((2,)), dma((QC + 3,)), dma((G,)),
         ],
         compiler_params=pltpu.CompilerParams(
             collective_id=0, has_side_effects=True, vmem_limit_bytes=56 * 2**20
         ),
-    )(tokens, norm_gain, value_w, gate_w, taps.transpose(1, 0, 2), cgain, out_w, fgain.reshape(1, width))
+    )(tokens, norm_gain, value_w, gate_w, taps.transpose(1, 0, 2), cgain, out_w)
+    step = rows // EPILOGUE
+    return pl.pallas_call(
+        scale_rows,
+        grid=(EPILOGUE,),
+        out_shape=jax.ShapeDtypeStruct((rows, width), bf16),
+        in_specs=[
+            pl.BlockSpec((step, width), lambda i: (i, 0)),
+            pl.BlockSpec((step, 1), lambda i: (i, 0)),
+            pl.BlockSpec((1, width), lambda i: (0, 0)),
+        ],
+        out_specs=pl.BlockSpec((step, width), lambda i: (i, 0)),
+        compiler_params=pltpu.CompilerParams(vmem_limit_bytes=60 * 2**20),
+    )(x, scale, fgain.reshape(1, width))
 
 
 def tokens_f32(tokens, xg, t):

time: 98.7 us -> 98 us (level)
  local copies, waits for them, and re-layouts: 1.87 us -> 0 us
  Pallas kernels: 96.6 us -> 97.8 us
    unnamed x1 -> x0, local copies, waits for them, and re-layouts: 1.87 us -> none
    pallas_call x1 -> x2, Pallas kernels: 96.6 us -> 97.8 us  [the longest x1 95.9 us: quad_on_device(): pl.pallas_call(functools.partial(quad_kernel, G, n, T, L), out_shape=(jax...]
where the time goes in v4:
time: 98 us; the launch traced here: 97.8 us
  Pallas kernels  97.8 us (100%)
    pallas_call x1, Pallas kernels, quad_on_device(): pl.pallas_call(functools.partial(quad_kernel, G, n, T, L), out_shape=(jax...  95.9 us

profile of v4, /device:TPU:0, one launch (start us, length us, event | category | flops | bytes accessed | tf_op | source)
XLA Modules:
  0.0 97.8 jit_solution(11266093949914258914)
XLA Ops:
  0.0 95.9 %shard_map.82 = (bf16[256,1024]{1,0:T(8,128)(2,1)}, f32[256,1]{1,0:T(8,128)}) custom-call(bf16[256,1024]{1,0:T(8,128)(2,1)} %tokens.1, f32[2,4096]{1,0:T(2,128)} %gain_hbm.1, bf16[2,1024,256]{2,1,0:T(8,128)(2,1)} %value_w.1, bf16[2,1024,256]{2,1,0:T(8,128)(2,1)} %gate_w.1, f32[31,2,256]{2,1,0:T(2,128)} %bitcast.2, f32[2,256]{1,0:T(2,128)} %cgain_hbm.1, ...), custom_call_target="tpu_custom_call" | custom-call | tf_op jit(solution)/shard_map/pallas_call | solution.py:1292
  95.9 2.0 %shard_map.83 = bf16[256,1024]{1,0:T(8,128)(2,1)} custom-call(bf16[256,1024]{1,0:T(8,128)(2,1)} %get-tuple-element.7.x, f32[256,1]{1,0:T(8,128)} %get-tuple-element.8.scale, f32[1,1024]{1,0:T(1,128)} %bitcast.3), custom_call_target="tpu_custom_call" | custom-call | tf_op jit(solution)/shard_map/pallas_call | solution.py:1324

commit v5 on v4

--- a/solution.py
+++ b/solution.py
@@ -527,8 +527,9 @@
     result[...] = (x_state[...] * scale * fgain[...]).astype(bf16)
 
 
-QC = 4
+QC = 8
 RC = 4
+XC = 4
 EPILOGUE = 2
 
 
@@ -536,7 +537,7 @@
     G, n, T, L,
     tokens, gain_hbm, value_w, gate_w, taps_hbm, cgain_hbm, out_w,
     x_out, scale_out,
-    wvg, wo, xg, xn, glu_out, acc, pad, padf, convg, act, stat, x_state, leaving, gain, taps, cgain,
+    wvg, wo, xg, xn, glu_out, acc, pad, padf, convg, act, column, stat, x_state, leaving, gain, taps, cgain,
     local_sem, recv_z, recv_o, send_w, x_sem, e_sem, c_sem, s_sem, h_sem, hs_sem, g_sem, f_sem, o_sem,
 ):
     g, s, t = lax.axis_index("grp"), lax.axis_index("sp"), lax.axis_index("tp")
@@ -553,7 +554,7 @@
     pieces = QC + RC
     size = {"vg": depth // QC, "wo": out_rows // RC}
     count = {"vg": QC, "wo": RC}
-    shared_from = QC - 1
+    shared_from = 3 * QC // 4
     f32, bf16 = jnp.float32, jnp.bfloat16
     last = n - 1
     low = s < n // 2
@@ -563,7 +564,7 @@
     outer = jnp.where(low, s - 1, s + 1)
     edge, mine, near, far = (jnp.where(low, a, last - a) for a in (0, 1, n - 2, n - 1))
     other = lax.rem(g + 1, G)
-    x_chunks = QC
+    x_chunks = XC
     x_rows = rows // x_chunks
     own = pl.ds(PAD, rows)
     first_vg, first_wo, second_vg, second_wo = (0, "vg"), (0, "wo"), (1, "vg"), (1, "wo")
@@ -680,7 +681,8 @@
     def across(stage, q, j, send=Y):
         r = piece(stage, q, g, j)
         return pltpu.make_async_remote_copy(
-            src_ref=r, dst_ref=r, send_sem=send_w.at[send], recv_sem=recv_o.at[order_of(stage)],
+            src_ref=r, dst_ref=r, send_sem=send_w.at[send],
+            recv_sem=recv_o.at[2 * L if stage == second_vg and j is far else order_of(stage)],
             device_id={"grp": other}, device_id_type=MESH)
 
     def direct(stage, q):
@@ -693,7 +695,11 @@
         layer, kind = stage
         per = depth if kind == "vg" else out_rows
         ref = wvg if kind == "vg" else wo
-        wait_bytes(ref.at[layer, 0, pl.ds(0, (n - 1) * per)], recv_o.at[order_of(stage)])
+        blocks = n - 2 if stage == second_vg else n - 1
+        wait_bytes(ref.at[layer, 0, pl.ds(0, blocks * per)], recv_o.at[order_of(stage)])
+
+    def far_arrived():
+        wait_bytes(wvg.at[1, 0, pl.ds(0, depth)], recv_o.at[2 * L])
 
     def end_rows(c, target):
         src = pl.ds(pl.multiple_of(PAD + c * x_rows, PAD), x_rows)
@@ -790,9 +796,9 @@
                       lambda k: hs_sem.at[layer, side, k])
 
     def conv_spread(layer, part_):
-        part = pl.ds(part_ * (rows // 2), rows // 2)
-        return Spread(lambda j: convg.at[layer, j, part], convg.at[layer, pl.ds(0, 3), part],
-                      convg.at[layer, pl.ds(0, 2), part], lambda k: c_sem.at[layer, part_, k])
+        cols = channels_of(g if part_ == 0 else other)
+        return Spread(lambda j: convg.at[layer, j, :, cols], convg.at[layer, pl.ds(0, 3), :, cols],
+                      convg.at[layer, pl.ds(0, 2), :, cols], lambda k: c_sem.at[layer, part_, k])
 
     def to_peers(buf, sem, k):
         for d in range(1, T):
@@ -800,16 +806,7 @@
                 src_ref=buf.at[0], dst_ref=buf.at[d], send_sem=sem.at[k], recv_sem=sem.at[k + 1],
                 device_id={"tp": lax.rem(t + d, T)}, device_id_type=MESH).start()
 
-    def columns_of(index_):
-        wait_bytes(stat.at[index_, pl.ds(0, T - 1)], s_sem.at[2 * index_ + 1])
-        got = jnp.concatenate([stat[index_, d] for d in range(T)] + [jnp.zeros((128 - 8 * T, rows), f32)], axis=0)
-        return got.T
-
-    def share(index_, columns):
-        lane = lax.broadcasted_iota(jnp.int32, (rows, 128), 1)
-        tile = jnp.zeros((rows, 128), f32)
-        for i, column in enumerate(columns):
-            tile = jnp.where(lane == i, column, tile)
+    def share(index_, tile):
         stat[index_, 0] = tile.T[:8, :]
         to_peers(stat.at[index_], s_sem, 2 * index_)
 
@@ -827,22 +824,24 @@
             return carry
         lax.fori_loop(0, T, body, 0)
 
-    def project(layer, held, start, size_, into, h):
-        def body(j, carry):
+    def project(layer, held, start, size_, into, h, part="whole"):
+        def body(k, carry):
+            j = lax.rem(far + 1 + k, T)
             block = wvg[layer, h, pl.ds(pl.multiple_of(j * width, width), width), :]
-            part = jnp.dot(xn[held, j, start:start + size_, :], block, preferred_element_type=f32)
-
-            @pl.when(j == 0)
-            def _():
-                acc[start:start + size_, :] = part
-
-            @pl.when(j > 0)
-            def _():
-                acc[start:start + size_, :] += part
+            term = jnp.dot(xn[held, j, start:start + size_, :], block, preferred_element_type=f32)
+
+            @pl.when(k == 0)
+            def _():
+                acc[start:start + size_, :] = term
+
+            @pl.when(k > 0)
+            def _():
+                acc[start:start + size_, :] += term
             return carry
-        lax.fori_loop(0, T, body, 0)
-        glu = acc[start:start + size_, :half] * jax.nn.sigmoid(acc[start:start + size_, half:])
-        into[start:start + size_, pl.ds(pl.multiple_of(h * half, half), half)] = glu.astype(bf16)
+        lax.fori_loop(T - 1 if part == "late" else 0, T - 1 if part == "early" else T, body, 0)
+        if part != "early":
+            glu = acc[start:start + size_, :half] * jax.nn.sigmoid(acc[start:start + size_, half:])
+            into[start:start + size_, pl.ds(pl.multiple_of(h * half, half), half)] = glu.astype(bf16)
 
     def x_right(layer):
         return pltpu.make_async_remote_copy(
@@ -890,37 +889,52 @@
             pl.when(from_left)(lambda: getattr(halo_spread(layer, 0), do)())
             pl.when(from_right)(lambda: getattr(halo_spread(layer, 1), do)())
 
-    def convolve(layer, between):
-        padf[...] = pad[layer].astype(f32)
+    def channels_of(h):
+        return pl.ds(pl.multiple_of(h * half, half), half)
+
+    def convolve(layer, h, turn):
+        @pl.when(s >= 0)
+        def _():
+            rows_of(layer, h, turn)
+        if turn == G - 1:
+            share(layer, column[...])
+        conv_spread(layer, turn).begin()
+
+    def rows_of(layer, h, turn):
+        cols = channels_of(h)
+        padf[...] = pad[layer, :, cols].astype(f32)
         block = 64
-        sums, squares = [], []
         for r in range(0, rows, block):
-            total = jnp.zeros((block, chans), f32)
+            total = jnp.zeros((block, half), f32)
             for k in range(n_taps):
                 start = r + PAD - reach + k
-                total = total + taps[k, layer:layer + 1, :] * padf[start:start + block, :]
-            mean = jnp.sum(total, axis=1, keepdims=True) / chans
+                total = total + taps[k, layer:layer + 1, cols] * padf[start:start + block, :]
+            mean = jnp.sum(total, axis=1, keepdims=True) / half
             shifted = total - mean
-            convg[layer, t, r:r + block, :] = shifted.astype(bf16)
-            sums.append(mean)
-            squares.append(jnp.sum(shifted * shifted, axis=1, keepdims=True))
-            if r + block == rows // 2:
-                conv_spread(layer, 0).begin()
-                between()
-        share(layer, [jnp.concatenate(sums, 0), jnp.concatenate(squares, 0)])
-        conv_spread(layer, 1).begin()
+            convg[layer, t, r:r + block, cols] = shifted.astype(bf16)
+            lane = lax.broadcasted_iota(jnp.int32, (block, 128), 1)
+            before = column[r:r + block, :] if turn else jnp.zeros((block, 128), f32)
+            squares = jnp.sum(shifted * shifted, axis=1, keepdims=True)
+            column[r:r + block, :] = jnp.where(lane == 2 * h, mean, jnp.where(lane == 2 * h + 1, squares, before))
 
     def activate(layer):
-        got = columns_of(layer)
-        means = [got[:, 8 * d:8 * d + 1] for d in range(T)]
-        center = sum(means[1:], means[0]) / T
-        apart = [m - center for m in means]
-        square = sum((got[:, 8 * d + 1:8 * d + 2] + chans * (apart[d] * apart[d]) for d in range(T)), jnp.zeros((rows, 1), f32))
-        scale = lax.rsqrt(square / C + 1e-05)
+        wait_bytes(stat.at[layer, pl.ds(0, T - 1)], s_sem.at[2 * layer + 1])
+        got = [stat[layer, d] for d in range(T)]
+        pairs = [(rows_[2 * h:2 * h + 1, :], rows_[2 * h + 1:2 * h + 2, :]) for rows_ in got for h in range(G)]
+        center = sum((m for m, _ in pairs[1:]), pairs[0][0]) / (T * G)
+        away = [m - center for m, _ in pairs]
+        square = jnp.zeros((1, rows), f32)
+        for a, (_, sq) in zip(away, pairs):
+            square = square + (sq + half * (a * a))
+        lines = away + [lax.rsqrt(square / C + 1e-05)]
+        table = jnp.concatenate(lines + [jnp.zeros((128 - len(lines), rows), f32)], axis=0).T
+        scale = table[:, T * G:T * G + 1]
         for d in range(T):
             j = lax.rem(t + T - d, T)
             by = cgain[j, layer:layer + 1, :]
-            normal = (convg[layer, j].astype(f32) + apart[d]) * scale
+            apart = jnp.concatenate(
+                [jnp.broadcast_to(table[:, i:i + 1], (rows, half)) for i in range(G * d, G * (d + 1))], axis=1)
+            normal = (convg[layer, j].astype(f32) + apart) * scale
             act[j] = jax.nn.silu(normal * by).astype(bf16)
 
     def add_branch(layer, h):
@@ -1020,14 +1034,14 @@
             normalize(0, 0, 0, 0, full)
 
     def second_chunks(q):
-        from_inner(first_vg, q, far)
+        each(q * QC // x_chunks, (q + 1) * QC // x_chunks, lambda k: from_inner(first_vg, k, far))
 
         @pl.when(is_mid)
         def _():
             wait_bytes(xg.at[0, t, pl.ds(0, x_rows)], f_sem.at[2 + q])
             edge_spread(q).begin()
     with scope("B_vg0_far"):
-        each(0, QC, second_chunks)
+        each(0, x_chunks, second_chunks)
 
     @pl.when(is_mid)
     def _():
@@ -1040,7 +1054,7 @@
     with scope("C1_wo0_near"):
         each(RC // 2, RC, lambda q: from_inner(first_wo, q, near))
     edge_relays(x_chunks - 1, x_chunks)
-    push_in(second_vg, QC // 2, QC // 2 + 1)
+    push_in(second_vg, QC // 2, 3 * QC // 4)
     end_sends("in", second_vg, QC // 2, QC)
 
     @pl.when(is_mid)
@@ -1049,11 +1063,13 @@
             each(0, x_chunks, lambda c: edge_spread(c).complete())
         with scope("norm_e"):
             normalize(0, L, 1, PAD, rows)
+    with scope("D1_vg1_near"):
+        each(0 * QC // 4, (0 + 1) * QC // 4, lambda q: from_inner(second_vg, q, near))
+
+    @pl.when(is_mid)
+    def _():
         with scope("proj0e_g"):
             project(0, 1, PAD, rows, glu_out, g)
-
-    with scope("D1_vg1_near"):
-        from_inner(second_vg, 0, near)
 
     @pl.when(is_mid)
     def _():
@@ -1063,6 +1079,8 @@
             project(0, 1, PAD, rows, glu_out, other)
     with scope("C2_wo0_edge"):
         each(0, RC // 2, lambda q: from_edge(first_wo, q))
+    with scope("D1_vg1_near"):
+        each(QC // 4, QC // 2, lambda q: from_inner(second_vg, q, near))
 
     @pl.when(is_mid)
     def _():
@@ -1087,11 +1105,9 @@
     def _():
         end_glu(edge).start()
 
-    with scope("D1_vg1_near"):
-        each(1, QC // 2, lambda q: from_inner(second_vg, q, near))
     with scope("C2_wo0_edge"):
         each(RC // 2, RC, lambda q: from_edge(first_wo, q))
-    push_in(second_vg, QC // 2 + 1, QC)
+    push_in(second_vg, 3 * QC // 4, QC)
     end_sends("in", second_wo, 0, RC)
 
     @pl.when(is_end)
@@ -1100,9 +1116,10 @@
             wait_bytes(glu_out, f_sem.at[2 + x_chunks])
 
     with scope("conv0"):
-        convolve(0, lambda: None)
+        convolve(0, g, 0)
+        convolve(0, other, 1)
     with scope("D2_vg1_edge"):
-        from_edge(second_vg, 0)
+        each(0 * QC // 4, (0 + 1) * QC // 4, lambda q: from_edge(second_vg, q))
     with scope("C3_wo0_far"):
         each(0, RC // 2, lambda q: from_inner(first_wo, q, far))
     with scope("conv0_relay"):
@@ -1120,7 +1137,7 @@
     with scope("act0"):
         activate(0)
     with scope("D2_vg1_edge"):
-        from_edge(second_vg, 1)
+        each(1 * QC // 4, (1 + 1) * QC // 4, lambda q: from_edge(second_vg, q))
     push_in(second_wo, 0, RC // 2)
 
     def next_x(h, turn):
@@ -1131,7 +1148,7 @@
     with scope("out0_g"):
         next_x(g, 0)
     with scope("D2_vg1_near"):
-        from_inner(second_vg, QC // 2, near)
+        each(QC // 2, 3 * QC // 4, lambda q: from_inner(second_vg, q, near))
     with scope("wait_wo0"):
         others_arrived(first_wo)
     with scope("out0"):
@@ -1140,22 +1157,24 @@
     end_sends("direct", second_vg, 0, QC)
     end_sends("direct", second_wo, 0, RC)
     with scope("D3_vg1_near"):
-        each(QC // 2 + 1, QC, lambda q: from_inner(second_vg, q, near))
+        each(3 * QC // 4, QC, lambda q: from_inner(second_vg, q, near))
     with scope("D3_vg1_edge"):
-        from_edge(second_vg, 2)
+        each(2 * QC // 4, (2 + 1) * QC // 4, lambda q: from_edge(second_vg, q))
     with scope("D4_vg1_far"):
-        from_inner(second_vg, 0, far)
+        each(0 * QC // 4, (0 + 1) * QC // 4, lambda q: from_inner(second_vg, q, far))
     with scope("D3_vg1_edge"):
-        each(3, QC, lambda q: from_edge(second_vg, q))
+        each(3 * QC // 4, QC, lambda q: from_edge(second_vg, q))
     push_in(second_wo, RC // 2, RC)
     with scope("D4_vg1_far"):
-        from_inner(second_vg, 1, far)
+        each(1 * QC // 4, (1 + 1) * QC // 4, lambda q: from_inner(second_vg, q, far))
     with scope("x1_relay"):
         half_spread(g, 0).relay()
+    with scope("E1_near"):
+        each(0, RC // 2, lambda q: from_inner(second_wo, q, near))
     with scope("halo1_begin"):
         pl.when(is_end)(lambda: halo(1, "begin"))
     with scope("D4_vg1_far"):
-        from_inner(second_vg, 2, far)
+        each(2 * QC // 4, (2 + 1) * QC // 4, lambda q: from_inner(second_vg, q, far))
     with scope("x1_relay"):
         pl.when(is_end)(half_spread(other, 1).relay)
     with scope("halo1_relay"):
@@ -1163,15 +1182,15 @@
     with scope("E1_wo1_edge"):
         each(0, RC // 2, lambda q: from_edge(second_wo, q))
     with scope("D4_vg1_far"):
-        each(3, QC, lambda q: from_inner(second_vg, q, far))
+        pl.when(is_mid)(lambda: each(3 * QC // 4, QC, lambda q: from_inner(second_vg, q, far)))
     with scope("E1_wo1_edge"):
         each(RC // 2, RC, lambda q: from_edge(second_wo, q))
     with scope("halo1_begin"):
         pl.when(is_mid)(lambda: halo(1, "begin"))
     with scope("x1_relay"):
         pl.when(is_mid)(half_spread(other, 1).relay)
-    with scope("E1_wo1_near"):
-        pl.when(is_mid)(lambda: each(0, RC // 2, lambda q: from_inner(second_wo, q, near)))
+    with scope("E1_near"):
+        pl.when(is_mid)(lambda: each(RC // 2, RC, lambda q: from_inner(second_wo, q, near)))
     with scope("halo1_relay"):
         pl.when(is_mid)(lambda: halo(1, "relay"))
     with scope("x1_complete"):
@@ -1180,30 +1199,39 @@
         halo(1, "complete")
     with scope("norm1"):
         normalize(1, 1, 0, 0, full)
-    with scope("E1_wo1_near"):
-        pl.when(is_mid)(lambda: each(RC // 2, RC, lambda q: from_inner(second_wo, q, near)))
+    with scope("D4_vg1_far"):
+        pl.when(is_end)(lambda: each(3 * QC // 4, QC, lambda q: from_inner(second_vg, q, far)))
+    with scope("E2_m"):
+        pl.when(is_mid)(lambda: each(0, RC // 2, lambda q: from_inner(second_wo, q, far)))
     with scope("proj1_g"):
         project(1, 0, 0, full, pad.at[1], g)
+    with scope("conv1_g"):
+        convolve(1, g, 0)
     with scope("E2_m"):
-        pl.when(is_mid)(lambda: each(0, RC // 2, lambda q: from_inner(second_wo, q, far)))
+        pl.when(is_mid)(lambda: each(RC // 2, RC, lambda q: from_inner(second_wo, q, far)))
     with scope("E1_e"):
-        pl.when(is_end)(lambda: each(0, RC // 2, lambda q: from_inner(second_wo, q, near)))
+        pl.when(is_end)(lambda: each(RC // 2, 3 * RC // 4, lambda q: from_inner(second_wo, q, near)))
     with scope("wait_vg1"):
         others_arrived(second_vg)
     with scope("proj1"):
-        project(1, 0, 0, full, pad.at[1], other)
+        project(1, 0, 0, full, pad.at[1], other, "early")
     with scope("E1_e"):
-        pl.when(is_end)(lambda: each(RC // 2, RC, lambda q: from_inner(second_wo, q, near)))
-    with scope("E2_m"):
-        pl.when(is_mid)(lambda: each(RC // 2, RC, lambda q: from_inner(second_wo, q, far)))
+        pl.when(is_end)(lambda: each(3 * RC // 4, RC, lambda q: from_inner(second_wo, q, near)))
+    def far_chunk(k):
+        with scope("E2_e"):
+            pl.when(is_end)(lambda: each(k * RC // 4, (k + 1) * RC // 4, lambda q: from_inner(second_wo, q, far)))
+    far_chunk(0)
+    with scope("wait_vg1_far"):
+        far_arrived()
+    far_chunk(1)
+    with scope("proj1_far"):
+        project(1, 0, 0, full, pad.at[1], other, "late")
     with scope("conv1"):
-        convolve(1, lambda: None)
-    with scope("E2_e"):
-        pl.when(is_end)(lambda: each(0, RC // 2, lambda q: from_inner(second_wo, q, far)))
+        convolve(1, other, 1)
+    far_chunk(2)
+    far_chunk(3)
     with scope("conv1_relay"):
         conv_spread(1, 0).relay()
-    with scope("E2_e"):
-        pl.when(is_end)(lambda: each(RC // 2, RC, lambda q: from_inner(second_wo, q, far)))
     with scope("conv1_relay"):
         conv_spread(1, 1).relay()
     with scope("conv1_gather"):
@@ -1224,7 +1252,7 @@
     with scope("out1"):
         last_x(other, 1)
     xf = x_state[...]
-    share(L, [jnp.sum(xf * xf, axis=1, keepdims=True)])
+    share(L, jnp.broadcast_to(jnp.sum(xf * xf, axis=1, keepdims=True), (rows, 128)))
 
     halo(0, "drain")
     halo(1, "drain")
@@ -1264,10 +1292,11 @@
         sent_twice(3 * later // 2, Y)
 
     with scope("final_stat"):
-        got = columns_of(L)
+        wait_bytes(stat.at[L, pl.ds(0, T - 1)], s_sem.at[2 * L + 1])
         for index_ in range(L + 1):
             wait_bytes(stat.at[index_, pl.ds(0, T - 1)], s_sem.at[2 * index_])
-    total = sum((got[:, 8 * d:8 * d + 1] for d in range(1, T)), got[:, 0:1])
+    line = sum((stat[L, d, 0:1, :] for d in range(1, T)), stat[L, 0, 0:1, :])
+    total = jnp.broadcast_to(line, (128, rows)).T[:, 0:1]
     scale_out[...] = lax.rsqrt(total / D + 1e-06)
     for turn in range(G):
         wait_bytes(leaving.at[:, pl.ds(0, out_half)], o_sem.at[turn])
@@ -1302,9 +1331,10 @@
             pltpu.VMEM((full, chans), bf16),
             pltpu.VMEM((full, 2 * chans // G), f32),
             pltpu.VMEM((L, full, chans), bf16),
-            pltpu.VMEM((full, chans), f32),
+            pltpu.VMEM((full, chans // G), f32),
             pltpu.VMEM((L, T, rows, chans), bf16),
             pltpu.VMEM((T, rows, chans), bf16),
+            pltpu.VMEM((rows, 128), f32),
             pltpu.VMEM((L + 1, T, 8, rows), f32),
             pltpu.VMEM((rows, width), f32),
             pltpu.VMEM((rows, width), bf16),
@@ -1312,9 +1342,9 @@
             pltpu.VMEM((taps.shape[1], L, chans), f32),
             pltpu.VMEM((T,) + cgain.shape, f32),
             dma((2 * L + 4,)),
-            dma((L * (QC + RC), 3)), dma((2 * L,)), dma((5,)),
-            dma((1 + G, 3)), dma((QC, 3)), dma((L, 2, 3)), dma((2 * (L + 1),)),
-            dma((L, 4)), dma((L, 2, 3)), dma((2,)), dma((QC + 3,)), dma((G,)),
+            dma((L * (QC + RC), 3)), dma((2 * L + 1,)), dma((5,)),
+            dma((1 + G, 3)), dma((XC, 3)), dma((L, 2, 3)), dma((2 * (L + 1),)),
+            dma((L, 4)), dma((L, 2, 3)), dma((2,)), dma((XC + 3,)), dma((G,)),
         ],
         compiler_params=pltpu.CompilerParams(
             collective_id=0, has_side_effects=True, vmem_limit_bytes=56 * 2**20

time: 98 us -> 97.1 us (level)
  no operation moved by 1% of the time
where the time goes in v5:
time: 97.1 us; the launch traced here: 97 us
  Pallas kernels  97 us (100%)
    pallas_call x1, Pallas kernels, quad_on_device(): pl.pallas_call(functools.partial(quad_kernel, G, n, T, L), out_shape=(jax...  95 us
    pallas_call x1, Pallas kernels, quad_on_device(): pl.pallas_call(scale_rows, grid=(EPILOGUE,), out_shape=jax.ShapeDtypeStru...  1.96 us

profile of v5, /device:TPU:0, one launch (start us, length us, event | category | flops | bytes accessed | tf_op | source)
XLA Modules:
  0.0 97.0 jit_solution(3349509545298279718)
XLA Ops:
  0.0 95.0 %shard_map.82 = (bf16[256,1024]{1,0:T(8,128)(2,1)}, f32[256,1]{1,0:T(8,128)}) custom-call(bf16[256,1024]{1,0:T(8,128)(2,1)} %tokens.1, f32[2,4096]{1,0:T(2,128)} %gain_hbm.1, bf16[2,1024,256]{2,1,0:T(8,128)(2,1)} %value_w.1, bf16[2,1024,256]{2,1,0:T(8,128)(2,1)} %gate_w.1, f32[31,2,256]{2,1,0:T(2,128)} %bitcast.2, f32[2,256]{1,0:T(2,128)} %cgain_hbm.1, ...), custom_call_target="tpu_custom_call" | custom-call | tf_op jit(solution)/shard_map/pallas_call | solution.py:1321
  95.0 2.0 %shard_map.83 = bf16[256,1024]{1,0:T(8,128)(2,1)} custom-call(bf16[256,1024]{1,0:T(8,128)(2,1)} %get-tuple-element.7.x, f32[256,1]{1,0:T(8,128)} %get-tuple-element.8.scale, f32[1,1024]{1,0:T(1,128)} %bitcast.3), custom_call_target="tpu_custom_call" | custom-call | tf_op jit(solution)/shard_map/pallas_call | solution.py:1354

commit v6 on v5

--- a/solution.py
+++ b/solution.py
@@ -1243,16 +1243,20 @@
     def last_x(h, turn):
         add_branch(1, h)
         cols = half_columns(h)
-        leaving[:, cols] = x_state[:, cols].astype(bf16)
+        xf = x_state[:, cols]
+        leaving[:, cols] = xf.astype(bf16)
         pltpu.make_async_copy(leaving.at[:, cols], x_out.at[:, cols], o_sem.at[turn]).start()
+        squares = jnp.broadcast_to(jnp.sum(xf * xf, axis=1, keepdims=True), (rows, 128))
+        if turn < G - 1:
+            column[...] = squares
+        else:
+            share(L, column[...] + squares)
     with scope("out1_g"):
         last_x(g, 0)
     with scope("wait_wo1"):
         others_arrived(second_wo)
     with scope("out1"):
         last_x(other, 1)
-    xf = x_state[...]
-    share(L, jnp.broadcast_to(jnp.sum(xf * xf, axis=1, keepdims=True), (rows, 128)))
 
     halo(0, "drain")
     halo(1, "drain")

time: 97.1 us -> 97 us (level)
  no operation moved by 1% of the time
where the time goes in v6:
time: 97 us; the launch traced here: 96.8 us
  Pallas kernels  96.8 us (100%)
    pallas_call x1, Pallas kernels, quad_on_device(): pl.pallas_call(functools.partial(quad_kernel, G, n, T, L), out_shape=(jax...  94.8 us
    pallas_call x1, Pallas kernels, quad_on_device(): pl.pallas_call(scale_rows, grid=(EPILOGUE,), out_shape=jax.ShapeDtypeStru...  1.96 us

profile of v6, /device:TPU:0, one launch (start us, length us, event | category | flops | bytes accessed | tf_op | source)
XLA Modules:
  0.0 96.8 jit_solution(17731853105957365195)
XLA Ops:
  0.0 94.8 %shard_map.82 = (bf16[256,1024]{1,0:T(8,128)(2,1)}, f32[256,1]{1,0:T(8,128)}) custom-call(bf16[256,1024]{1,0:T(8,128)(2,1)} %tokens.1, f32[2,4096]{1,0:T(2,128)} %gain_hbm.1, bf16[2,1024,256]{2,1,0:T(8,128)(2,1)} %value_w.1, bf16[2,1024,256]{2,1,0:T(8,128)(2,1)} %gate_w.1, f32[31,2,256]{2,1,0:T(2,128)} %bitcast.2, f32[2,256]{1,0:T(2,128)} %cgain_hbm.1, ...), custom_call_target="tpu_custom_call" | custom-call | tf_op jit(solution)/shard_map/pallas_call | solution.py:1325
  94.9 2.0 %shard_map.83 = bf16[256,1024]{1,0:T(8,128)(2,1)} custom-call(bf16[256,1024]{1,0:T(8,128)(2,1)} %get-tuple-element.7.x, f32[256,1]{1,0:T(8,128)} %get-tuple-element.8.scale, f32[1,1024]{1,0:T(1,128)} %bitcast.3), custom_call_target="tpu_custom_call" | custom-call | tf_op jit(solution)/shard_map/pallas_call | solution.py:1358
